TPU v7x, 128 devices: a whole 4x4x4 slice. The times are simulated.
128 devices in a mesh: rep: 2 (over z_hi), fs: 32 (over z_lo, y, x), tp: 2 (over core).
Axes of the slice: x: 4, y: 4, z: 4 (z_hi: 2, z_lo: 2; z = z_hi * 2 + z_lo), core: 2. Of those that a mesh axis runs over, the one named last changes fastest.
Arguments:
- tokens: bfloat16 [64, 1024, 2048], P(('rep', 'fs'), 'tp'), may hold values from -6 to 6
- mix_gain: float32 [2048], replicated, may hold values from 0.1 to 1.9
- out_gate_w: float32 [2048, 1024], P('fs', 'tp'), may hold values from -0.125 to 0.125
- in_gate_w: float32 [2048, 1024], P('fs', 'tp'), may hold values from -0.125 to 0.125
- value_w: float32 [2048, 1024], P('fs', 'tp'), may hold values from -0.125 to 0.125
- out_gate_scale: float32 [1024], P(('tp', 'fs')), may hold values from 0.28 to 3.5
- in_gate_scale: float32 [1024], P(('tp', 'fs')), may hold values from 0.5 to 2
- value_scale: float32 [1024], P(('tp', 'fs')), may hold values from 0.5 to 2
- mix_taps: float32 [3, 1024], P(None, 'tp'), may hold values from -3.5 to 3.5
- conv_gain: float32 [1024], P('tp'), may hold values from 0.1 to 1.9
- out_proj_w: float32 [1024, 2048], P('tp', 'fs'), may hold values from -0.1875 to 0.1875
- proj_scale: float32 [2048], P('fs'), may hold values from 0.5 to 2
- ffn_gain: float32 [2048], replicated, may hold values from 0.1 to 1.9
- gate_w: float32 [2048, 2816], P('fs', 'tp'), may hold values from -0.125 to 0.125
- up_w: float32 [2048, 2816], P('fs', 'tp'), may hold values from -0.125 to 0.125
- gate_scale: float32 [2816], P(('tp', 'fs')), may hold values from 0.5 to 2
- up_scale: float32 [2816], P(('tp', 'fs')), may hold values from 0.5 to 2
- gate_taps: float32 [3, 2816], P(None, 'tp'), may hold values from -3.5 to 3.5
- up_taps: float32 [3, 2816], P(None, 'tp'), may hold values from -3.5 to 3.5
- gate_bias: float32 [2816], P('tp'), may hold values from -3 to 3
- up_bias: float32 [2816], P('tp'), may hold values from -3 to 3
- down_w: float32 [2816, 2048], P('tp', 'fs'), may hold values from -0.109375 to 0.109375
- down_scale: float32 [2048], P('fs'), may hold values from 0.5 to 2
Outputs:
- layer_out: bfloat16 [64, 1024, 2048], P(('rep', 'fs'), 'tp')
All inputs are finite; a program needn't handle non-finite values.
Results may differ from a plain program's by a relative error of at most 0.02.
Values may be sent and summed in bfloat16 or wider, within the bound.
A program may use at most 128 MiB of HBM per device.

v0:
```python
import jax
import jax.numpy as jnp
from jax import lax
from jax.experimental import pallas as pl
from jax.experimental.pallas import tpu as pltpu
from jax.sharding import PartitionSpec as P

epsilon = 1e-06
MESH = pl.DeviceIdType.MESH
UNIT = 256
TURNED = "so"

TREES = {
    "A": (
        ((), "x+", 1),
        ((), "x-", 1),
        ("s01", "xs", 1),
        ((0, 1, 2), "y+", 4),
        ((0, 1, 2), "y-", 4),
        ((0, 1, 2), "zs", 4),
        ("s34", "ys", 4),
        ("s34", "zo", 4),
        ("o34", "zo", 4),
        ((6,), "zs", 4),
    ),
    "D": (
        ((), "zs", 1),
        ((0,), "y+", 2),
        ((0,), "y-", 2),
        ("s12", "ys", 2),
        ((1, 2, 3), "x+", 8),
        ((1, 2, 3), "x-", 8),
        ((4,), "x+", 4),
        ((5,), "x-", 4),
    ),
}


def needs_of(kind, m, turn):
    need = TREES[kind][m][0]
    if isinstance(need, str):
        first, second = int(need[1]), int(need[2])
        return (first if (turn > 0) == (need[0] == "s") else second,)
    return need


def link_of(kind, m, turn):
    name = TREES[kind][m][1]
    sign = {"+": 1, "-": -1, "s": turn, "o": -turn}[name[1]]
    return name[0], sign


def plan(chunks, comps, rate=44.0, hop=2.2, issue=0.04, ahead=4.0):
    links = {(a, s): 0.0 for a in "xyz" for s in (1, -1)}
    arrive, waited, sent, ops, done, t = {}, set(), set(), [], {}, 0.0
    every = [(c, m) for c in range(len(chunks)) for m in range(len(TREES[chunks[c][0]]))]
    log = []

    def wait(pairs):
        for pair in pairs:
            if pair not in waited:
                waited.add(pair)
                ops.append(("wait", *pair))

    while True:
        best = None
        for c, m in every:
            kind, turn, size = chunks[c]
            if (c, m) in sent:
                continue
            needs = [(c, k) for k in needs_of(kind, m, turn)]
            link = link_of(kind, m, turn)
            if all(arrive.get(k, 1e9) <= t for k in needs) and links[link] <= t + ahead:
                best = (c, m, needs, link, size * TREES[kind][m][2])
                break
        if best is not None:
            c, m, needs, link, size = best
            wait(needs)
            ops.append(("send", c, m))
            sent.add((c, m))
            t += issue
            links[link] = max(t, links[link]) + size / rate / 1000.0
            arrive[c, m] = links[link] + hop
            continue
        soon = []
        for k, (us, of_chunks, of_comps) in enumerate(comps):
            if k in done:
                continue
            pairs = [(c, m) for c, m in every if c in of_chunks]
            ready = max([arrive.get(q, 1e9) for q in pairs] + [done.get(b, 1e9) + lag for b, lag in of_comps] + [0.0])
            if ready <= t:
                wait(pairs)
                ops.append(("comp", k))
                log.append((round(t, 1), k))
                t += us
                done[k] = t
                break
            if ready < 1e8:
                soon.append(ready)
        else:
            later = [a for a in arrive.values() if a > t] + [b - ahead for b in links.values() if b - ahead > t] + soon
            if not later:
                break
            t = min(later) + 1e-6
    wait(every)
    return ops, t, log, arrive


def list_of_chunks(n_mix, n_pj, n_gu, n_dn):
    item = 64 * UNIT * 2
    chunks, where, count = [("A", 1, 4096)], [("sc", 0, 128)], {"A": 0, "D": 0}

    def add(name, kinds, units):
        for i, kind in enumerate(kinds):
            width = min(1.0, units - i)
            turn = 1 if count[kind] % 2 == 0 else -1
            count[kind] += 1
            chunks.append((kind, turn, int(item * width)))
            where.append((name, i, int(UNIT * width)))

    add("mix", "ADAADA", n_mix)
    add("pj", "AD", n_pj)
    add("gu", "ADAADAADAAD", n_gu)
    add("dn", "ADADAA", n_dn)
    return chunks, where


CHUNKS, WHERE = list_of_chunks(6, 2, 11, 5.5)
CHUNK_OF = {(name, i): c for c, (name, i, _) in enumerate(WHERE)}
ROWS = 256


def list_of_blocks():
    names, comps, number = [], [], {}

    def add(name, us, chunks=(), after=()):
        number[name] = len(names)
        names.append(name)
        comps.append((us, {CHUNK_OF[c] for c in chunks}, [(number[b], lag) for b, lag in after]))

    add(("norm",), 2.5)
    add(("scales",), 1.0, [("sc", 0)])
    for k in range(6):
        add(("mix", k), 1.5, [("mix", k)], [(("norm",), 4.0), (("scales",), 0.0)])
    for g in range(2):
        add(("conv", g), 1.2, [], [(("mix", 3 * g + i), 0.0) for i in range(3)] + [(("conv", 0), 0.0)] * g)
    add(("proj", 0), 1.3, [("pj", 0), ("pj", 1)], [(("conv", 0), 0.0), (("conv", 1), 0.0)])
    add(("proj", 1), 1.3, [], [(("proj", 0), 0.0)])
    add(("first",), 2.5, [], [(("proj", 1), 3.0)])
    for k in range(11):
        add(("gu", k), 2.2, [("gu", k)], [(("first",), 4.0)])
    for j in range(6):
        add(("down", j), 1.5, [("dn", j)], [(("gu", k), 0.0) for k in (2 * j, 2 * j + 1) if k < 11] + ([(("down", j - 1), 0.0)] if j else []))
    add(("last",), 3.0, [], [(("down", 5), 3.0)])
    return names, comps


def place():
    rep, fs = lax.axis_index("rep"), lax.axis_index("fs")
    tp = lax.axis_index("tp")
    x, y, zl = lax.rem(fs, 4), lax.rem(fs // 4, 4), fs // 16
    z = rep * 2 + zl
    xs = {n: lax.rem(x + 4 + n, 4) for n in (-1, 1, 2)} | {0: x}
    ys = {n: lax.rem(y + 4 + n, 4) for n in (-1, 1, 2)} | {0: y}
    near = {}
    for sign in (1, -1):
        near["x", sign] = (rep, zl * 16 + y * 4 + xs[sign], tp)
        near["y", sign] = (rep, zl * 16 + ys[sign] * 4 + x, tp)
        zn = lax.rem(z + 4 + sign, 4)
        near["z", sign] = (zn // 2, lax.rem(zn, 2) * 16 + y * 4 + x, tp)
    return xs, ys, {0: zl, 1: 1 - zl}, near, (rep, fs, 1 - tp), tp


def carried(kind, m, turn, arriving):
    sent = {
        "A": (
            (0, 0, 0),
            (0, 0, 0),
            (0, 0, -turn),
            (0, 0, None),
            (0, 0, None),
            (0, 0, None),
            (0, -turn, None),
            (0, -turn, None),
            (0, turn, None),
            (0, 2, None),
        ),
        "D": (
            (0, 0, 0),
            (None, 0, 0),
            (None, 0, 0),
            (None, -turn, 0),
            (None, None, 0),
            (None, None, 0),
            ("plane0", None, -1),
            ("plane1", None, 1),
        ),
    }[kind][m]
    if not arriving:
        return sent
    link, sign = link_of(kind, m, turn)
    z, y, x = sent

    def back(v, n):
        v = v - n
        return v + 4 if v < -1 else v - 4 if v > 2 else v

    if link == "x":
        x = back(x, sign)
    elif link == "y":
        y = back(y, sign)
    else:
        z = 1 - z
    return z, y, x


def mega_kernel(
    ops, names, tokens, mix_in, pj_in, gu_in, dn_in, sc_in, mix_gain, ffn_gain, mix_taps, conv_gain, gate_taps, up_taps,
    gate_bias, up_bias, out, mix, pj, gu, dn, sc, tok, rows, gates, conv, square, acc, hidden, psend, precv, sqrecv, sv_mix,
    sv_gu, sv_pj, sv_dn, own_sem, send_sem, recv_sem, side_send, side_recv, out_sem,
):
    f32, bf16 = jnp.float32, jnp.bfloat16
    xs, ys, zs, near, other, tp = place()
    bufs = {"mix": mix, "pj": pj, "gu": gu, "dn": dn, "sc": sc}
    x, y, zl = xs[0], ys[0], zs[0]
    mine = pl.multiple_of(tp * 512, 512)
    yours = pl.multiple_of((1 - tp) * 512, 512)
    own = [
        pltpu.make_async_copy(sc_in, sc.at[zl, y, x], own_sem.at[0]),
        pltpu.make_async_copy(mix_in, mix.at[:, zl, y, x], own_sem.at[1]),
        pltpu.make_async_copy(pj_in, pj.at[zl, y, x], own_sem.at[2]),
        pltpu.make_async_copy(tokens, tok, own_sem.at[3]),
        pltpu.make_async_copy(gu_in, gu.at[:, zl, y, x], own_sem.at[4]),
        pltpu.make_async_copy(dn_in, dn.at[zl, y, x], own_sem.at[5]),
    ]
    for copy in own:
        copy.start()
    barrier = pltpu.get_barrier_semaphore()
    for device in [*near.values(), other]:
        pl.semaphore_signal(barrier, inc=1, device_id=device, device_id_type=MESH)
    pl.semaphore_wait(barrier, 7)
    for copy in own:
        copy.wait()

    def part(c, at):
        name, i, width = WHERE[c]
        z, y, x = at
        z = slice(None) if z is None else int(z[-1]) if isinstance(z, str) else zs[z]
        y = slice(None) if y is None else ys[y]
        x = slice(None) if x is None else xs[x]
        ref = bufs[name]
        if name in ("mix", "gu"):
            return ref.at[i, z, y, x]
        if name == "sc":
            return ref.at[z, y, x]
        return ref.at[z, y, x, :, i * UNIT : i * UNIT + width]

    def copy_of(c, m, arriving):
        kind, turn, _ = CHUNKS[c]
        ref = part(c, carried(kind, m, turn, arriving))
        return pltpu.make_async_remote_copy(
            src_ref=ref,
            dst_ref=ref,
            send_sem=send_sem.at[c],
            recv_sem=recv_sem.at[c, m],
            device_id=near[link_of(kind, m, turn)],
            device_id_type=MESH,
        )

    def to_other(src, dst, i):
        return pltpu.make_async_remote_copy(
            src_ref=src, dst_ref=dst, send_sem=side_send.at[i], recv_sem=side_recv.at[i], device_id=other, device_id_type=MESH
        )

    def normed(values, gain):
        return (values * lax.rsqrt(jnp.mean(values * values, axis=1, keepdims=True) + epsilon) * gain[...]).astype(bf16)

    def shifted(values, before):
        both = jnp.concatenate([before, values], axis=0)
        return pltpu.roll(both, 1, 0)[8:], pltpu.roll(both, 2, 0)[8:]

    def dot_nt(left, right):
        return lax.dot_general(left, right, (((1,), (1,)), ((), ())), preferred_element_type=f32)

    def spread(row, width, group):
        total = jnp.zeros((1, 128), f32)
        lane = lax.broadcasted_iota(jnp.int32, (1, 128), 1)
        for s in range(group * 128 // width, min(31, (group * 128 + 127) // width) + 1):
            at = s * width - group * 128
            line = sc[s // 16, s // 4 % 4, s % 4, row : row + 1, :]
            if at % 128:
                line = pltpu.roll(line, at % 128, 1)
            total = jnp.where((lane >= at) & (lane < at + width), line, total)
        return total

    send_rows = [to_other(rows.at[pl.ds(mine, 512)], rows.at[pl.ds(mine, 512)], i) for i in (0, 3)]
    recv_rows = [to_other(rows.at[pl.ds(yours, 512)], rows.at[pl.ds(yours, 512)], i) for i in (0, 3)]
    send_sums = [to_other(psend, precv, i) for i in (1, 4)]
    send_square = to_other(square.at[pl.ds(yours, 512)], sqrecv, 2)
    seen = set()

    def block_norm():
        @pl.loop(0, 512, step=64)
        def _(r):
            at = pl.multiple_of(r, 64)
            rows[pl.ds(mine + at, 64), :] = normed(tok[pl.ds(at, 64), :].astype(f32), mix_gain)

        send_rows[0].start()

    def block_scales():
        for k in range(6):
            for i in range(2):
                sv_mix[k, :, 128 * i : 128 * i + 128] = spread(k % 3, 16, k // 3 * 2 + i)
        for k in range(11):
            sv_gu[k, :, :128] = spread(3, 44, k)
            sv_gu[k, :, 128:] = spread(4, 44, k)
        for k in range(16):
            sv_pj[k // 4, :, 128 * (k % 4) : 128 * (k % 4) + 128] = spread(5, 64, k)
            sv_dn[k // 4, :, 128 * (k % 4) : 128 * (k % 4) + 128] = spread(6, 64, k)

    def block_mix(k):
        if "rows" not in seen:
            seen.add("rows")
            recv_rows[0].wait_recv()

        @pl.loop(0, 1024, step=ROWS)
        def _(r):
            at = pl.ds(pl.multiple_of(r, ROWS), ROWS)
            weight = mix[k].reshape(2048, 256)
            gates[k, at, :] = (jnp.dot(rows[at, :], weight, preferred_element_type=f32) * sv_mix[k]).astype(bf16)

    def block_conv(g):
        cols = slice(256 * g, 256 * g + 256)
        taps, gain = mix_taps[:, cols], conv_gain[:, cols]

        def body(i, before):
            at = pl.ds(pl.multiple_of(i * 128, 128), 128)
            value = gates[3 * g, at, :].astype(f32) * gates[3 * g + 1, at, :].astype(f32)
            one, two = shifted(value, before)
            total = taps[0:1] * two + taps[1:2] * one + taps[2:3] * value
            done = (gates[3 * g + 2, at, :].astype(f32) * total).astype(bf16).astype(f32)
            conv[at, cols] = (done * gain).astype(bf16)
            squares = jnp.broadcast_to(jnp.sum(done * done, axis=1, keepdims=True), (128, 128))
            square[at, :] = squares if g == 0 else square[at, :] + squares
            return value[-8:]

        lax.fori_loop(0, 8, body, jnp.zeros((8, 256), f32))
        if g == 1:
            send_square.start()

    def block_proj(half):
        start = yours if half == 0 else mine

        @pl.loop(0, 8)
        def _(i):
            r, n = pl.multiple_of(i // 4 * ROWS, ROWS), i % 4
            weight = pj[n // 2, pl.ds(n % 2 * 2, 2)].reshape(512, 512)
            part_sum = dot_nt(conv[pl.ds(start + r, ROWS), :], weight) * sv_pj[n]
            cols = pl.ds(pl.multiple_of(n * 512, 512), 512)
            if half == 0:
                psend[pl.ds(r, ROWS), cols] = part_sum.astype(bf16)
            else:
                acc[pl.ds(start + r, ROWS), cols] = part_sum

        if half == 0:
            send_sums[0].start()

    def block_first():
        send_sums[0].wait_recv()
        send_square.wait_recv()
        send_rows[0].wait_send()

        @pl.loop(0, 512, step=64)
        def _(r):
            at = pl.ds(pl.multiple_of(r, 64), 64)
            there = pl.ds(pl.multiple_of(mine + r, 64), 64)
            squares = square[there, :1] + sqrecv[at, :1]
            summed = (acc[there, :] + precv[at, :].astype(f32)) * lax.rsqrt(squares / 1024 + epsilon)
            first = (tok[at, :].astype(f32) + summed).astype(bf16)
            tok[at, :] = first
            rows[there, :] = normed(first.astype(f32), ffn_gain)

        send_rows[1].start()

    def block_gu(k):
        if "rows2" not in seen:
            seen.add("rows2")
            recv_rows[1].wait_recv()
        cols = slice(128 * k, 128 * k + 128)

        def body(i, before):
            at = pl.ds(pl.multiple_of(i * ROWS, ROWS), ROWS)
            weight = gu[k].reshape(2048, 256)
            pre = (jnp.dot(rows[at, :], weight, preferred_element_type=f32) * sv_gu[k]).astype(bf16).astype(f32)
            one, two = shifted(pre, before)
            acts = []
            for j, (taps, bias) in enumerate(((gate_taps, gate_bias), (up_taps, up_bias))):
                half, t = slice(128 * j, 128 * j + 128), taps[:, cols]
                acts.append(t[0:1] * two[:, half] + t[1:2] * one[:, half] + t[2:3] * pre[:, half] + bias[:, cols])
            hidden[at, cols] = (acts[0] / (1.0 + jnp.exp(-acts[0])) * acts[1]).astype(bf16)
            return pre[-8:]

        lax.fori_loop(0, 1024 // ROWS, body, jnp.zeros((8, 256), f32))

    def block_down(j):
        width = WHERE[CHUNK_OF["dn", j]][2]
        lanes = slice(UNIT * j, UNIT * j + width)

        def product(r, n):
            weight = dn[n // 2, pl.ds(n % 2 * 2, 2), :, :, lanes].reshape(512, width)
            return dot_nt(hidden[pl.ds(r, ROWS), lanes], weight)

        def sweep(first, count, store):
            @pl.loop(0, count * 4)
            def _(i):
                r, n = pl.multiple_of(first + i // 4 * ROWS, ROWS), i % 4
                cols = pl.ds(pl.multiple_of(n * 512, 512), 512)
                store(i // 4 * ROWS, r, n, cols)

        if j < 5:

            def store(_, r, n, cols):
                value = product(r, n)
                acc[pl.ds(r, ROWS), cols] = value if j == 0 else acc[pl.ds(r, ROWS), cols] + value

            sweep(0, 4, store)
            return
        send_sums[0].wait_send()

        def give(here, r, n, cols):
            value = (acc[pl.ds(r, ROWS), cols] + product(r, n)) * sv_dn[n]
            psend[pl.ds(pl.multiple_of(here, ROWS), ROWS), cols] = value.astype(bf16)

        sweep(yours, 2, give)
        send_sums[1].start()

        def keep(_, r, n, cols):
            acc[pl.ds(r, ROWS), cols] = (acc[pl.ds(r, ROWS), cols] + product(r, n)) * sv_dn[n]

        sweep(mine, 2, keep)

    def block_last():
        send_sums[1].wait_recv()
        send_rows[1].wait_send()
        outs = []
        for q in range(4):

            @pl.loop(0, 128, step=64)
            def _(r):
                at = pl.ds(pl.multiple_of(q * 128 + r, 64), 64)
                there = pl.ds(pl.multiple_of(mine + q * 128 + r, 64), 64)
                summed = acc[there, :] + precv[at, :].astype(f32)
                rows[there, :] = (tok[at, :].astype(f32) + summed).astype(bf16)

            outs.append(
                pltpu.make_async_copy(rows.at[pl.ds(mine + q * 128, 128)], out.at[pl.ds(q * 128, 128)], out_sem.at[q])
            )
            outs[-1].start()
        for copy in outs:
            copy.wait()

    blocks = {
        "norm": block_norm, "scales": block_scales, "mix": block_mix, "conv": block_conv, "proj": block_proj,
        "first": block_first, "gu": block_gu, "down": block_down, "last": block_last,
    }
    for op in ops:
        if op[0] == "send":
            copy_of(op[1], op[2], False).start()
        elif op[0] == "wait":
            copy_of(op[1], op[2], True).wait_recv()
        else:
            name, *index = names[op[1]]
            blocks[name](*index)
    for c, (kind, turn, _) in enumerate(CHUNKS):
        for m in range(len(TREES[kind])):
            copy_of(c, m, False).wait_send()
    send_square.wait_send()
    send_sums[1].wait_send()


def mega(*args):
    names, comps = list_of_blocks()
    ops, _, _, _ = plan(CHUNKS, comps)
    f32, bf16 = jnp.float32, jnp.bfloat16
    hbm, vmem = pl.BlockSpec(memory_space=pl.ANY), pl.BlockSpec(memory_space=pltpu.VMEM)
    dma = pltpu.SemaphoreType.DMA
    return pl.pallas_call(
        lambda *refs: mega_kernel(ops, names, *refs),
        out_shape=jax.ShapeDtypeStruct((512, 2048), bf16),
        in_specs=[hbm] * 6 + [vmem] * 8,
        out_specs=hbm,
        scratch_shapes=[
            pltpu.VMEM((6, 2, 4, 4, 64, 256), bf16),
            pltpu.VMEM((2, 4, 4, 64, 512), bf16),
            pltpu.VMEM((11, 2, 4, 4, 64, 256), bf16),
            pltpu.VMEM((2, 4, 4, 64, 1408), bf16),
            pltpu.VMEM((2, 4, 4, 8, 128), f32),
            pltpu.VMEM((512, 2048), bf16),
            pltpu.VMEM((1024, 2048), bf16),
            pltpu.VMEM((6, 1024, 256), bf16),
            pltpu.VMEM((1024, 512), bf16),
            pltpu.VMEM((1024, 128), f32),
            pltpu.VMEM((1024, 2048), f32),
            pltpu.VMEM((1024, 1408), bf16),
            pltpu.VMEM((512, 2048), bf16),
            pltpu.VMEM((512, 2048), bf16),
            pltpu.VMEM((512, 128), f32),
            pltpu.VMEM((6, 1, 256), f32),
            pltpu.VMEM((11, 1, 256), f32),
            pltpu.VMEM((4, 1, 512), f32),
            pltpu.VMEM((4, 1, 512), f32),
            dma((6,)),
            dma((len(CHUNKS),)),
            dma((len(CHUNKS), 10)),
            dma((5,)),
            dma((5,)),
            dma((4,)),
        ],
        compiler_params=pltpu.CompilerParams(collective_id=0, has_side_effects=True, vmem_limit_bytes=62 * 1024 * 1024),
    )(*args)


def local(
    tokens, mix_gain, out_gate_w, in_gate_w, value_w, out_gate_scale, in_gate_scale, value_scale, mix_taps, conv_gain,
    out_proj_w, proj_scale, ffn_gain, gate_w, up_w, gate_scale, up_scale, gate_taps, up_taps, gate_bias, up_bias, down_w,
    down_scale,
):
    f32, bf16 = jnp.float32, jnp.bfloat16
    mix_own = jnp.stack(
        [w.astype(bf16)[:, 256 * g : 256 * g + 256] for g in (0, 1) for w in (in_gate_w, value_w, out_gate_w)]
    )
    gu_own = jnp.stack(
        [
            jnp.concatenate([w[:, 128 * k : 128 * k + 128] for w in (gate_w, up_w)], axis=1).astype(bf16)
            for k in range(11)
        ]
    )
    pj_own = out_proj_w.astype(bf16).T
    dn_own = down_w.astype(bf16).T
    sc_own = jnp.stack(
        [
            jnp.pad(s, (0, 128 - s.shape[0]))
            for s in (in_gate_scale, value_scale, out_gate_scale, gate_scale, up_scale, proj_scale, down_scale)
        ]
        + [jnp.zeros(128, f32)]
    )
    line = lambda v: v.reshape(1, -1)
    return mega(
        tokens[0], mix_own, pj_own, gu_own, dn_own, sc_own, line(mix_gain), line(ffn_gain), mix_taps, line(conv_gain),
        gate_taps, up_taps, line(gate_bias), line(up_bias),
    )[None]


def solution(mesh):
    placed = (
        P(("rep", "fs"), "tp", None), P(), P("fs", "tp"), P("fs", "tp"), P("fs", "tp"), P(("tp", "fs")), P(("tp", "fs")),
        P(("tp", "fs")), P(None, "tp"), P("tp"), P("tp", "fs"), P("fs"), P(), P("fs", "tp"), P("fs", "tp"), P(("tp", "fs")),
        P(("tp", "fs")), P(None, "tp"), P(None, "tp"), P("tp"), P("tp"), P("tp", "fs"), P("fs"),
    )
    return jax.shard_map(
        local, mesh=mesh, in_specs=placed, out_specs=P(("rep", "fs"), "tp", None), check_vma=False
    )
```

profile of v0, /device:TPU:1, one launch (start us, length us, event | category | flops | bytes accessed | tf_op | source)
XLA Modules:
  0.0 163.5 jit_solution(1108936336435522537)
XLA Ops:
  0.0 0.0 copy-start.1
  0.0 0.7 pad_bitcast_fusion.6
  0.7 0.7 pad_bitcast_fusion.4
  1.4 0.7 pad_bitcast_fusion
  2.1 0.7 pad_bitcast_fusion.2
  2.7 0.6 stack.74.refs_5_
  3.3 1.3 reshape.359.refs_12_
  4.6 1.3 reshape.360.refs_13_
  5.9 0.9 convert_element_type.118
  6.9 0.9 convert_element_type.116
  7.8 0.9 convert_element_type.117
  8.7 1.5 convert_bitcast_fusion.1.refs_2_
  10.2 1.0 convert.70
  11.3 1.0 convert.71
  12.3 0.0 copy-done.1
  12.3 0.7 convert_bitcast_fusion.refs_4_
  13.2 0.0 copy-start
  13.2 0.0 copy-start.2
  13.3 0.7 copy-done
  14.0 0.1 copy-done.2
  14.0 146.3 %shard_map.217 = bf16[512,2048]{1,0:T(8,128)(2,1)} custom-call(bf16[512,2048]{1,0:T(8,128)(2,1)} %bitcast.92, bf16[6,64,256]{2,1,0:T(8,128)(2,1)} %copy-done.2, bf16[64,512]{1,0:T(8,128)(2,1)} %convert_bitcast_fusion.1.refs_2_, bf16[11,64,256]{2,1,0:T(8,128)(2,1)} %copy-done, bf16[64,1408]{1,0:T(8,128)(2,1)} %convert_bitcast_fusion.refs_4_, ...), custom_call_target="tpu_custom_call" | custom-call | tf_op jit(solution)/shard_map/pallas_call | solution.py:487
  160.4 3.2 %copy.40 = bf16[1,512,2048]{2,1,0:T(8,128)(2,1)} copy(bf16[1,512,2048]{2,1,0:T(8,128)(2,1)} %bitcast.91) | data formatting | bytes 4194304
  (19 shorter events, 0.2 us)
Async XLA Ops:
  0.0 12.3 %copy-start.1 = (f32[1408,64]{0,1:T(8,128)S(1)}, f32[1408,64]{0,1:T(8,128)}, u32[]{:S(2)}) copy-start(f32[1408,64]{0,1:T(8,128)} %param.44) | copy-start | bytes 1081348
  13.2 0.7 copy-start
  13.2 0.8 copy-start.2
where the time goes:
time: 164 us
  Pallas kernels  146 us (89%)
  local copies, waits for them, and re-layouts  9.96 us (6%)
  other arithmetic  7.06 us (4%)
    pallas_call x1, Pallas kernels, mega(): pl.pallas_call(lambda *refs: mega_kernel(ops, names, *refs), out_shape=ja...  146 us
    unnamed x12, local copies, waits for them, and re-layouts  3.96 us
    another operation x6, local copies, waits for them, and re-layouts, local(): jnp.stack([jnp.pad(s, (0, 128 - s.shape[0])) for s in (in_gate_scale, val...  3.34 us

commit v1 on v0

--- a/solution.py
+++ b/solution.py
@@ -50,7 +50,10 @@
     return name[0], sign
 
 
-def plan(chunks, comps, rate=44.0, hop=2.2, issue=0.04, ahead=4.0):
+RATE, HOP, AHEAD = 45.0, 2.2, 3.0
+
+
+def plan(chunks, comps, own_after, rate=RATE, hop=HOP, issue=0.04, ahead=AHEAD):
     links = {(a, s): 0.0 for a in "xyz" for s in (1, -1)}
     arrive, waited, sent, ops, done, t = {}, set(), set(), [], {}, 0.0
     every = [(c, m) for c in range(len(chunks)) for m in range(len(TREES[chunks[c][0]]))]
@@ -70,7 +73,8 @@
                 continue
             needs = [(c, k) for k in needs_of(kind, m, turn)]
             link = link_of(kind, m, turn)
-            if all(arrive.get(k, 1e9) <= t for k in needs) and links[link] <= t + ahead:
+            here = bool(needs) or c not in own_after or own_after[c] in done
+            if here and all(arrive.get(k, 1e9) <= t for k in needs) and links[link] <= t + ahead:
                 best = (c, m, needs, link, size * TREES[kind][m][2])
                 break
         if best is not None:
@@ -128,6 +132,7 @@
 CHUNKS, WHERE = list_of_chunks(6, 2, 11, 5.5)
 CHUNK_OF = {(name, i): c for c, (name, i, _) in enumerate(WHERE)}
 ROWS = 256
+DOWN = ((0, 2), (2, 2), (4, 1), (5, 1))
 
 
 def list_of_blocks():
@@ -138,7 +143,9 @@
         names.append(name)
         comps.append((us, {CHUNK_OF[c] for c in chunks}, [(number[b], lag) for b, lag in after]))
 
-    add(("norm",), 2.5)
+    add(("cast", "gu"), 0.6)
+    add(("cast", "rest"), 0.4)
+    add(("norm",), 2.0)
     add(("scales",), 1.0, [("sc", 0)])
     for k in range(6):
         add(("mix", k), 1.5, [("mix", k)], [(("norm",), 4.0), (("scales",), 0.0)])
@@ -149,10 +156,16 @@
     add(("first",), 2.5, [], [(("proj", 1), 3.0)])
     for k in range(11):
         add(("gu", k), 2.2, [("gu", k)], [(("first",), 4.0)])
-    for j in range(6):
-        add(("down", j), 1.5, [("dn", j)], [(("gu", k), 0.0) for k in (2 * j, 2 * j + 1) if k < 11] + ([(("down", j - 1), 0.0)] if j else []))
-    add(("last",), 3.0, [], [(("down", 5), 3.0)])
-    return names, comps
+    for j, (first, count) in enumerate(DOWN):
+        units = range(first, first + count)
+        halves = [k for u in units for k in (2 * u, 2 * u + 1) if k < 11]
+        add(("down", j), 0.3 + 1.1 * count, [("dn", u) for u in units], [(("gu", k), 0.0) for k in halves] + ([(("down", j - 1), 0.0)] if j else []))
+    add(("last",), 3.0, [], [(("down", 3), 3.0)])
+    own_after = {}
+    for (name, _), c in CHUNK_OF.items():
+        if name in ("gu", "pj", "dn"):
+            own_after[c] = number["cast", "gu" if name == "gu" else "rest"]
+    return names, comps, own_after
 
 
 def place():
@@ -215,9 +228,9 @@
 
 
 def mega_kernel(
-    ops, names, tokens, mix_in, pj_in, gu_in, dn_in, sc_in, mix_gain, ffn_gain, mix_taps, conv_gain, gate_taps, up_taps,
-    gate_bias, up_bias, out, mix, pj, gu, dn, sc, tok, rows, gates, conv, square, acc, hidden, psend, precv, sqrecv, sv_mix,
-    sv_gu, sv_pj, sv_dn, own_sem, send_sem, recv_sem, side_send, side_recv, out_sem,
+    ops, names, tokens, in_w, val_w, out_w, gate_w, up_w, pj_w, dn_w, in_s, val_s, out_s, gate_s, up_s, pj_s, dn_s, mix_gain,
+    ffn_gain, mix_taps, conv_gain, gate_taps, up_taps, gate_bias, up_bias, out, mix, pj, gu, dn, sc, tok, rows, gates, conv, square, acc, hidden, psend, precv, sqrecv, sv_mix,
+    sv_gu, sv_pj, sv_dn, own_sem, send_sem, recv_sem, side_send, side_recv,
 ):
     f32, bf16 = jnp.float32, jnp.bfloat16
     xs, ys, zs, near, other, tp = place()
@@ -225,22 +238,43 @@
     x, y, zl = xs[0], ys[0], zs[0]
     mine = pl.multiple_of(tp * 512, 512)
     yours = pl.multiple_of((1 - tp) * 512, 512)
+    mix_f32 = [acc.at[64 * i : 64 * i + 64, 0:512] for i in range(3)]
+    gu_f32 = [acc.at[192 + 64 * i : 256 + 64 * i, 0:1408] for i in range(2)]
+    pj_f32, dn_f32 = acc.at[320:384, 0:512], acc.at[384:448, 0:1408]
     own = [
-        pltpu.make_async_copy(sc_in, sc.at[zl, y, x], own_sem.at[0]),
-        pltpu.make_async_copy(mix_in, mix.at[:, zl, y, x], own_sem.at[1]),
-        pltpu.make_async_copy(pj_in, pj.at[zl, y, x], own_sem.at[2]),
-        pltpu.make_async_copy(tokens, tok, own_sem.at[3]),
-        pltpu.make_async_copy(gu_in, gu.at[:, zl, y, x], own_sem.at[4]),
-        pltpu.make_async_copy(dn_in, dn.at[zl, y, x], own_sem.at[5]),
+        pltpu.make_async_copy(src, dst, own_sem.at[i])
+        for i, (src, dst) in enumerate(
+            zip(
+                (in_w, val_w, out_w, gate_w, up_w, pj_w, dn_w, tokens),
+                (*mix_f32, *gu_f32, pj_f32, dn_f32, tok),
+            )
+        )
     ]
     for copy in own:
         copy.start()
     barrier = pltpu.get_barrier_semaphore()
     for device in [*near.values(), other]:
         pl.semaphore_signal(barrier, inc=1, device_id=device, device_id_type=MESH)
+    sc[zl, y, x] = jnp.zeros((8, 128), f32)
+    for i, ref in enumerate((in_s, val_s, out_s, gate_s, up_s, pj_s, dn_s)):
+        sc[zl, y, x, i : i + 1, : ref.shape[0]] = ref[...].reshape(1, -1)
+    for i in range(3):
+        own[i].wait()
+        for g in range(2):
+            mix[3 * g + i, zl, y, x] = mix_f32[i][:, 256 * g : 256 * g + 256].astype(bf16)
     pl.semaphore_wait(barrier, 7)
-    for copy in own:
-        copy.wait()
+
+    def block_cast(which):
+        if which == "gu":
+            for i in range(2):
+                own[3 + i].wait()
+                for k in range(11):
+                    gu[k, zl, y, x, :, 128 * i : 128 * i + 128] = gu_f32[i][:, 128 * k : 128 * k + 128].astype(bf16)
+        else:
+            own[5].wait()
+            pj[zl, y, x] = pj_f32[...].astype(bf16)
+            own[6].wait()
+            dn[zl, y, x] = dn_f32[...].astype(bf16)
 
     def part(c, at):
         name, i, width = WHERE[c]
@@ -273,7 +307,7 @@
         )
 
     def normed(values, gain):
-        return (values * lax.rsqrt(jnp.mean(values * values, axis=1, keepdims=True) + epsilon) * gain[...]).astype(bf16)
+        return (values * lax.rsqrt(jnp.mean(values * values, axis=1, keepdims=True) + epsilon) * gain[...].reshape(1, -1)).astype(bf16)
 
     def shifted(values, before):
         both = jnp.concatenate([before, values], axis=0)
@@ -300,6 +334,8 @@
     seen = set()
 
     def block_norm():
+        own[7].wait()
+
         @pl.loop(0, 512, step=64)
         def _(r):
             at = pl.multiple_of(r, 64)
@@ -315,23 +351,22 @@
             sv_gu[k, :, :128] = spread(3, 44, k)
             sv_gu[k, :, 128:] = spread(4, 44, k)
         for k in range(16):
-            sv_pj[k // 4, :, 128 * (k % 4) : 128 * (k % 4) + 128] = spread(5, 64, k)
-            sv_dn[k // 4, :, 128 * (k % 4) : 128 * (k % 4) + 128] = spread(6, 64, k)
+            sv_pj[k // 2, :, 128 * (k % 2) : 128 * (k % 2) + 128] = spread(5, 64, k)
+            sv_dn[k // 2, :, 128 * (k % 2) : 128 * (k % 2) + 128] = spread(6, 64, k)
 
     def block_mix(k):
         if "rows" not in seen:
             seen.add("rows")
             recv_rows[0].wait_recv()
 
-        @pl.loop(0, 1024, step=ROWS)
-        def _(r):
-            at = pl.ds(pl.multiple_of(r, ROWS), ROWS)
+        for r in range(0, 1024, ROWS):
+            at = pl.ds(r, ROWS)
             weight = mix[k].reshape(2048, 256)
             gates[k, at, :] = (jnp.dot(rows[at, :], weight, preferred_element_type=f32) * sv_mix[k]).astype(bf16)
 
     def block_conv(g):
         cols = slice(256 * g, 256 * g + 256)
-        taps, gain = mix_taps[:, cols], conv_gain[:, cols]
+        taps, gain = mix_taps[:, cols], conv_gain[cols].reshape(1, 256)
 
         def body(i, before):
             at = pl.ds(pl.multiple_of(i * 128, 128), 128)
@@ -351,16 +386,14 @@
     def block_proj(half):
         start = yours if half == 0 else mine
 
-        @pl.loop(0, 8)
-        def _(i):
-            r, n = pl.multiple_of(i // 4 * ROWS, ROWS), i % 4
-            weight = pj[n // 2, pl.ds(n % 2 * 2, 2)].reshape(512, 512)
-            part_sum = dot_nt(conv[pl.ds(start + r, ROWS), :], weight) * sv_pj[n]
-            cols = pl.ds(pl.multiple_of(n * 512, 512), 512)
+        for n in range(8):
+            weight = pj[n // 4, n % 4].reshape(256, 512)
+            part_sum = dot_nt(conv[pl.ds(start, 512), :], weight) * sv_pj[n]
+            cols = slice(n * 256, n * 256 + 256)
             if half == 0:
-                psend[pl.ds(r, ROWS), cols] = part_sum.astype(bf16)
+                psend[:, cols] = part_sum.astype(bf16)
             else:
-                acc[pl.ds(start + r, ROWS), cols] = part_sum
+                acc[pl.ds(start, 512), cols] = part_sum
 
         if half == 0:
             send_sums[0].start()
@@ -389,60 +422,56 @@
         cols = slice(128 * k, 128 * k + 128)
 
         def body(i, before):
-            at = pl.ds(pl.multiple_of(i * ROWS, ROWS), ROWS)
+            at = pl.ds(i * ROWS, ROWS)
             weight = gu[k].reshape(2048, 256)
             pre = (jnp.dot(rows[at, :], weight, preferred_element_type=f32) * sv_gu[k]).astype(bf16).astype(f32)
             one, two = shifted(pre, before)
             acts = []
             for j, (taps, bias) in enumerate(((gate_taps, gate_bias), (up_taps, up_bias))):
                 half, t = slice(128 * j, 128 * j + 128), taps[:, cols]
-                acts.append(t[0:1] * two[:, half] + t[1:2] * one[:, half] + t[2:3] * pre[:, half] + bias[:, cols])
+                acts.append(t[0:1] * two[:, half] + t[1:2] * one[:, half] + t[2:3] * pre[:, half] + bias[cols].reshape(1, 128))
             hidden[at, cols] = (acts[0] / (1.0 + jnp.exp(-acts[0])) * acts[1]).astype(bf16)
             return pre[-8:]
 
-        lax.fori_loop(0, 1024 // ROWS, body, jnp.zeros((8, 256), f32))
+        before = jnp.zeros((8, 256), f32)
+        for i in range(1024 // ROWS):
+            before = body(i, before)
 
     def block_down(j):
-        width = WHERE[CHUNK_OF["dn", j]][2]
-        lanes = slice(UNIT * j, UNIT * j + width)
-
-        def product(r, n):
-            weight = dn[n // 2, pl.ds(n % 2 * 2, 2), :, :, lanes].reshape(512, width)
-            return dot_nt(hidden[pl.ds(r, ROWS), lanes], weight)
-
-        def sweep(first, count, store):
-            @pl.loop(0, count * 4)
-            def _(i):
-                r, n = pl.multiple_of(first + i // 4 * ROWS, ROWS), i % 4
-                cols = pl.ds(pl.multiple_of(n * 512, 512), 512)
-                store(i // 4 * ROWS, r, n, cols)
-
-        if j < 5:
-
-            def store(_, r, n, cols):
-                value = product(r, n)
-                acc[pl.ds(r, ROWS), cols] = value if j == 0 else acc[pl.ds(r, ROWS), cols] + value
-
-            sweep(0, 4, store)
+        first, count = DOWN[j]
+        width = sum(WHERE[CHUNK_OF["dn", u]][2] for u in range(first, first + count))
+        lanes = slice(UNIT * first, UNIT * first + width)
+
+        def product(start, count, n):
+            weight = dn[n // 4, n % 4, :, :, lanes].reshape(256, width)
+            return dot_nt(hidden[pl.ds(start, count), lanes], weight)
+
+        def sweep(start, count, store):
+            for n in range(8):
+                store(n, slice(n * 256, n * 256 + 256), pl.ds(start, count), product(start, count, n))
+
+        if j < len(DOWN) - 1:
+
+            def store(n, cols, at, value):
+                acc[at, cols] = value if j == 0 else acc[at, cols] + value
+
+            sweep(0, 1024, store)
             return
         send_sums[0].wait_send()
 
-        def give(here, r, n, cols):
-            value = (acc[pl.ds(r, ROWS), cols] + product(r, n)) * sv_dn[n]
-            psend[pl.ds(pl.multiple_of(here, ROWS), ROWS), cols] = value.astype(bf16)
-
-        sweep(yours, 2, give)
+        def give(n, cols, at, value):
+            psend[:, cols] = ((acc[at, cols] + value) * sv_dn[n]).astype(bf16)
+
+        sweep(yours, 512, give)
         send_sums[1].start()
 
-        def keep(_, r, n, cols):
-            acc[pl.ds(r, ROWS), cols] = (acc[pl.ds(r, ROWS), cols] + product(r, n)) * sv_dn[n]
-
-        sweep(mine, 2, keep)
+        def keep(n, cols, at, value):
+            acc[at, cols] = (acc[at, cols] + value) * sv_dn[n]
+
+        sweep(mine, 512, keep)
 
     def block_last():
         send_sums[1].wait_recv()
-        send_rows[1].wait_send()
-        outs = []
         for q in range(4):
 
             @pl.loop(0, 128, step=64)
@@ -450,16 +479,10 @@
                 at = pl.ds(pl.multiple_of(q * 128 + r, 64), 64)
                 there = pl.ds(pl.multiple_of(mine + q * 128 + r, 64), 64)
                 summed = acc[there, :] + precv[at, :].astype(f32)
-                rows[there, :] = (tok[at, :].astype(f32) + summed).astype(bf16)
-
-            outs.append(
-                pltpu.make_async_copy(rows.at[pl.ds(mine + q * 128, 128)], out.at[pl.ds(q * 128, 128)], out_sem.at[q])
-            )
-            outs[-1].start()
-        for copy in outs:
-            copy.wait()
+                out[at, :] = (tok[at, :].astype(f32) + summed).astype(bf16)
 
     blocks = {
+        "cast": block_cast,
         "norm": block_norm, "scales": block_scales, "mix": block_mix, "conv": block_conv, "proj": block_proj,
         "first": block_first, "gu": block_gu, "down": block_down, "last": block_last,
     }
@@ -475,20 +498,21 @@
         for m in range(len(TREES[kind])):
             copy_of(c, m, False).wait_send()
     send_square.wait_send()
+    send_rows[1].wait_send()
     send_sums[1].wait_send()
 
 
 def mega(*args):
-    names, comps = list_of_blocks()
-    ops, _, _, _ = plan(CHUNKS, comps)
+    names, comps, own_after = list_of_blocks()
+    ops, _, _, _ = plan(CHUNKS, comps, own_after)
     f32, bf16 = jnp.float32, jnp.bfloat16
     hbm, vmem = pl.BlockSpec(memory_space=pl.ANY), pl.BlockSpec(memory_space=pltpu.VMEM)
     dma = pltpu.SemaphoreType.DMA
     return pl.pallas_call(
         lambda *refs: mega_kernel(ops, names, *refs),
-        out_shape=jax.ShapeDtypeStruct((512, 2048), bf16),
-        in_specs=[hbm] * 6 + [vmem] * 8,
-        out_specs=hbm,
+        out_shape=pltpu.VMEM((512, 2048), bf16),
+        in_specs=[hbm] * 8 + [vmem] * 15,
+        out_specs=vmem,
         scratch_shapes=[
             pltpu.VMEM((6, 2, 4, 4, 64, 256), bf16),
             pltpu.VMEM((2, 4, 4, 64, 512), bf16),
@@ -507,17 +531,37 @@
             pltpu.VMEM((512, 128), f32),
             pltpu.VMEM((6, 1, 256), f32),
             pltpu.VMEM((11, 1, 256), f32),
-            pltpu.VMEM((4, 1, 512), f32),
-            pltpu.VMEM((4, 1, 512), f32),
-            dma((6,)),
+            pltpu.VMEM((8, 1, 256), f32),
+            pltpu.VMEM((8, 1, 256), f32),
+            dma((8,)),
             dma((len(CHUNKS),)),
             dma((len(CHUNKS), 10)),
             dma((5,)),
             dma((5,)),
-            dma((4,)),
         ],
-        compiler_params=pltpu.CompilerParams(collective_id=0, has_side_effects=True, vmem_limit_bytes=62 * 1024 * 1024),
+        compiler_params=pltpu.CompilerParams(collective_id=0, has_side_effects=True, vmem_limit_bytes=58 * 1024 * 1024),
     )(*args)
+
+
+def to_hbm(values):
+    def kernel(src, dst, sem):
+        copies = [
+            pltpu.make_async_copy(src.at[128 * q : 128 * q + 128], dst.at[128 * q : 128 * q + 128], sem.at[q])
+            for q in range(4)
+        ]
+        for copy in copies:
+            copy.start()
+        for copy in copies:
+            copy.wait()
+
+    return pl.pallas_call(
+        kernel,
+        out_shape=jax.ShapeDtypeStruct(values.shape, values.dtype),
+        in_specs=[pl.BlockSpec(memory_space=pltpu.VMEM)],
+        out_specs=pl.BlockSpec(memory_space=pl.ANY),
+        scratch_shapes=[pltpu.SemaphoreType.DMA((4,))],
+        compiler_params=pltpu.CompilerParams(vmem_limit_bytes=4 * 1024 * 1024),
+    )(values)
 
 
 def local(
@@ -525,30 +569,11 @@
     out_proj_w, proj_scale, ffn_gain, gate_w, up_w, gate_scale, up_scale, gate_taps, up_taps, gate_bias, up_bias, down_w,
     down_scale,
 ):
-    f32, bf16 = jnp.float32, jnp.bfloat16
-    mix_own = jnp.stack(
-        [w.astype(bf16)[:, 256 * g : 256 * g + 256] for g in (0, 1) for w in (in_gate_w, value_w, out_gate_w)]
-    )
-    gu_own = jnp.stack(
-        [
-            jnp.concatenate([w[:, 128 * k : 128 * k + 128] for w in (gate_w, up_w)], axis=1).astype(bf16)
-            for k in range(11)
-        ]
-    )
-    pj_own = out_proj_w.astype(bf16).T
-    dn_own = down_w.astype(bf16).T
-    sc_own = jnp.stack(
-        [
-            jnp.pad(s, (0, 128 - s.shape[0]))
-            for s in (in_gate_scale, value_scale, out_gate_scale, gate_scale, up_scale, proj_scale, down_scale)
-        ]
-        + [jnp.zeros(128, f32)]
-    )
-    line = lambda v: v.reshape(1, -1)
-    return mega(
-        tokens[0], mix_own, pj_own, gu_own, dn_own, sc_own, line(mix_gain), line(ffn_gain), mix_taps, line(conv_gain),
-        gate_taps, up_taps, line(gate_bias), line(up_bias),
-    )[None]
+    return to_hbm(mega(
+        tokens[0], in_gate_w, value_w, out_gate_w, gate_w, up_w, out_proj_w.T, down_w.T, in_gate_scale, value_scale,
+        out_gate_scale, gate_scale, up_scale, proj_scale, down_scale, mix_gain, ffn_gain, mix_taps, conv_gain, gate_taps,
+        up_taps, gate_bias, up_bias,
+    ))[None]
 
 
 def solution(mesh):

time: 164 us -> 128 us (0.78)
  Pallas kernels: 146 us -> 127 us
  local copies, waits for them, and re-layouts: 9.96 us -> 0 us
  other arithmetic: 7.06 us -> 0 us
    pallas_call x1 -> x2, Pallas kernels: 146 us -> 127 us  [the longest x1 126 us: mega(): pl.pallas_call(lambda *refs: mega_kernel(ops, names, *refs), out_shape=pl...]
    unnamed x12 -> x0, local copies, waits for them, and re-layouts: 3.96 us -> none
    another operation x6 -> x0, local copies, waits for them, and re-layouts: 3.34 us -> none  [local(): jnp.stack([jnp.pad(s, (0, 128 - s.shape[0])) for s in (in_gate_scale, val...]
    convert_element_type x3 -> x0, other arithmetic: 2.75 us -> none  [local(): w.astype(bf16)[:, 256 * g:256 * g + 256]]
    reshape x2 -> x0, local copies, waits for them, and re-layouts: 2.59 us -> none  [local(): line = lambda v: v.reshape(1, -1)]
    transpose x2 -> x0, other arithmetic: 2.22 us -> none  [the longest x1 1.53 us: local(): pj_own = out_proj_w.astype(bf16).T]
    another operation x3 -> x0, other arithmetic: 2.02 us -> none
where the time goes in v1:
time: 128 us; the launch traced here: 127 us
  Pallas kernels  127 us (99%)
    pallas_call x1, Pallas kernels, mega(): pl.pallas_call(lambda *refs: mega_kernel(ops, names, *refs), out_shape=pl...  126 us

profile of v1, /device:TPU:1, one launch (start us, length us, event | category | flops | bytes accessed | tf_op | source)
XLA Modules:
  0.0 127.4 jit_solution(11404533627341660782)
XLA Ops:
  0.0 125.9 %shard_map.217.src = bf16[512,2048]{1,0:T(8,128)(2,1)S(1)} custom-call(bf16[512,2048]{1,0:T(8,128)(2,1)} %bitcast.4, f32[64,512]{1,0:T(8,128)} %refs_1_.1, f32[64,512]{1,0:T(8,128)} %refs_2_.1, f32[64,512]{1,0:T(8,128)} %refs_3_.1, f32[64,1408]{1,0:T(8,128)} %refs_4_.1, f32[64,1408]{1,0:T(8,128)} %refs_5_.1, f32[64,512]{1,0:T(8,128)} %bitcast.6, ...), custom_call_target="tpu_custom_call" | custom-call | tf_op jit(solution)/shard_map/pallas_call | solution.py:511
  125.9 1.3 %shard_map.218 = bf16[512,2048]{1,0:T(8,128)(2,1)} custom-call(bf16[512,2048]{1,0:T(8,128)(2,1)S(1)} %shard_map.217.src), custom_call_target="tpu_custom_call" | custom-call | tf_op jit(solution)/shard_map/pallas_call | solution.py:557

commit v2 on v1

--- a/solution.py
+++ b/solution.py
@@ -33,6 +33,16 @@
         ((4,), "x+", 4),
         ((5,), "x-", 4),
     ),
+    "C": (
+        ((), "zs", 1),
+        ((0,), "x+", 2),
+        ((0,), "x-", 2),
+        ("s12", "xs", 2),
+        ((1, 2, 3), "y+", 8),
+        ((1, 2, 3), "y-", 8),
+        ((4,), "y+", 4),
+        ((5,), "y-", 4),
+    ),
 }
 
 
@@ -50,13 +60,42 @@
     return name[0], sign
 
 
-RATE, HOP, AHEAD = 45.0, 2.2, 3.0
+RATE, HOP, AHEAD = 46.0, 2.2, 2.5
+ORDER = (
+    ("mix", 5, "A", 1),
+    ("gu", 10, "D", 1),
+    ("mix", 0, "A", -1),
+    ("mix", 2, "A", 1),
+    ("mix", 1, "D", 1),
+    ("mix", 4, "D", -1),
+    ("gu", 8, "A", -1),
+    ("pj", 1, "D", -1),
+    ("mix", 3, "A", 1),
+    ("pj", 0, "A", 1),
+    ("gu", 6, "A", 1),
+    ("gu", 2, "A", -1),
+    ("gu", 3, "A", -1),
+    ("dn", 0, "D", -1),
+    ("gu", 1, "D", 1),
+    ("gu", 0, "A", 1),
+    ("dn", 1, "A", -1),
+    ("gu", 4, "D", 1),
+    ("gu", 9, "A", 1),
+    ("gu", 5, "A", -1),
+    ("gu", 7, "D", 1),
+    ("dn", 3, "A", 1),
+    ("dn", 4, "A", -1),
+    ("dn", 2, "D", -1),
+    ("dn", 5, "A", 1),
+)
+LEAD = {("A", 6): 1.0, ("C", 4): 12, ("D", 2): 0.5, ("D", 3): 9.0, ("D", 1): 6.0, ("D", 5): 3.5, ("D", 6): 10, ("A", 0): 0.5, ("D", 7): 8, ("D", 0): 4.0, ("A", 7): 1.5, ("C", 1): 5.0, ("A", 1): -3, ("A", 9): 3.0, ("A", 4): 1.0, ("A", 2): 9.0, ("A", 3): 0.5, ("C", 0): 1.5, ("D", 4): 6.0, ("C", 5): 9.5, ("C", 7): 8.0, ("C", 3): 1.5, ("A", 5): 1, ("C", 2): 8.0, ("A", 8): -0.5}
 
 
 def plan(chunks, comps, own_after, rate=RATE, hop=HOP, issue=0.04, ahead=AHEAD):
     links = {(a, s): 0.0 for a in "xyz" for s in (1, -1)}
     arrive, waited, sent, ops, done, t = {}, set(), set(), [], {}, 0.0
     every = [(c, m) for c in range(len(chunks)) for m in range(len(TREES[chunks[c][0]]))]
+    every.sort(key=lambda e: (e[0] - LEAD.get((chunks[e[0]][0], e[1]), 0.0), e[1]))
     log = []
 
     def wait(pairs):
@@ -110,29 +149,20 @@
     return ops, t, log, arrive
 
 
-def list_of_chunks(n_mix, n_pj, n_gu, n_dn):
-    item = 64 * UNIT * 2
-    chunks, where, count = [("A", 1, 4096)], [("sc", 0, 128)], {"A": 0, "D": 0}
-
-    def add(name, kinds, units):
-        for i, kind in enumerate(kinds):
-            width = min(1.0, units - i)
-            turn = 1 if count[kind] % 2 == 0 else -1
-            count[kind] += 1
-            chunks.append((kind, turn, int(item * width)))
-            where.append((name, i, int(UNIT * width)))
-
-    add("mix", "ADAADA", n_mix)
-    add("pj", "AD", n_pj)
-    add("gu", "ADAADAADAAD", n_gu)
-    add("dn", "ADADAA", n_dn)
+def list_of_chunks():
+    chunks, where = [("A", 1, 4096)], [("sc", 0, 128)]
+    for name, i, kind, turn in ORDER:
+        width = UNIT // 2 if (name, i) == LAST else UNIT
+        chunks.append((kind, turn, 64 * width * 2))
+        where.append((name, i, width))
     return chunks, where
 
 
-CHUNKS, WHERE = list_of_chunks(6, 2, 11, 5.5)
+LAST = ("dn", 5)
+CHUNKS, WHERE = list_of_chunks()
 CHUNK_OF = {(name, i): c for c, (name, i, _) in enumerate(WHERE)}
 ROWS = 256
-DOWN = ((0, 2), (2, 2), (4, 1), (5, 1))
+DOWN = ((0, 2), (2, 2), (4, 1))
 
 
 def list_of_blocks():
@@ -143,24 +173,26 @@
         names.append(name)
         comps.append((us, {CHUNK_OF[c] for c in chunks}, [(number[b], lag) for b, lag in after]))
 
-    add(("cast", "gu"), 0.6)
+    add(("cast", "gu"), 0.5)
     add(("cast", "rest"), 0.4)
-    add(("norm",), 2.0)
+    add(("norm",), 1.5)
     add(("scales",), 1.0, [("sc", 0)])
     for k in range(6):
-        add(("mix", k), 1.5, [("mix", k)], [(("norm",), 4.0), (("scales",), 0.0)])
+        add(("mix", k), 1.05, [("mix", k)], [(("norm",), 4.0), (("scales",), 0.0)])
     for g in range(2):
-        add(("conv", g), 1.2, [], [(("mix", 3 * g + i), 0.0) for i in range(3)] + [(("conv", 0), 0.0)] * g)
-    add(("proj", 0), 1.3, [("pj", 0), ("pj", 1)], [(("conv", 0), 0.0), (("conv", 1), 0.0)])
-    add(("proj", 1), 1.3, [], [(("proj", 0), 0.0)])
-    add(("first",), 2.5, [], [(("proj", 1), 3.0)])
+        add(("conv", g), 1.0, [], [(("mix", 3 * g + i), 0.0) for i in range(3)] + [(("conv", 0), 0.0)] * g)
+    add(("proj", 0), 0.8, [("pj", 0), ("pj", 1)], [(("conv", 0), 0.0), (("conv", 1), 0.0)])
+    add(("proj", 1), 0.8, [], [(("proj", 0), 0.0)])
+    add(("first",), 2.0, [], [(("proj", 1), 3.2)])
     for k in range(11):
-        add(("gu", k), 2.2, [("gu", k)], [(("first",), 4.0)])
+        add(("gu", k), 1.45, [("gu", k)], [(("first",), 4.0)])
     for j, (first, count) in enumerate(DOWN):
         units = range(first, first + count)
-        halves = [k for u in units for k in (2 * u, 2 * u + 1) if k < 11]
-        add(("down", j), 0.3 + 1.1 * count, [("dn", u) for u in units], [(("gu", k), 0.0) for k in halves] + ([(("down", j - 1), 0.0)] if j else []))
-    add(("last",), 3.0, [], [(("down", 3), 3.0)])
+        before = [(("gu", k), 0.0) for u in units for k in (2 * u, 2 * u + 1)] + [(("down", j - 1), 0.0)] * (j > 0)
+        add(("down", j), 0.1 + 1.15 * count, [("dn", u) for u in units], before)
+    add(("give",), 0.5, [], [(("down", len(DOWN) - 1), 0.0), (("gu", 10), 0.0)])
+    add(("base",), 1.3, [], [(("give",), 4.2)])
+    add(("final",), 2.2, [LAST], [(("base",), 0.0)])
     own_after = {}
     for (name, _), c in CHUNK_OF.items():
         if name in ("gu", "pj", "dn"):
@@ -208,6 +240,16 @@
             ("plane0", None, -1),
             ("plane1", None, 1),
         ),
+        "C": (
+            (0, 0, 0),
+            (None, 0, 0),
+            (None, 0, 0),
+            (None, 0, -turn),
+            (None, 0, None),
+            (None, 0, None),
+            ("plane0", -1, None),
+            ("plane1", 1, None),
+        ),
     }[kind][m]
     if not arriving:
         return sent
@@ -230,7 +272,7 @@
 def mega_kernel(
     ops, names, tokens, in_w, val_w, out_w, gate_w, up_w, pj_w, dn_w, in_s, val_s, out_s, gate_s, up_s, pj_s, dn_s, mix_gain,
     ffn_gain, mix_taps, conv_gain, gate_taps, up_taps, gate_bias, up_bias, out, mix, pj, gu, dn, sc, tok, rows, gates, conv, square, acc, hidden, psend, precv, sqrecv, sv_mix,
-    sv_gu, sv_pj, sv_dn, own_sem, send_sem, recv_sem, side_send, side_recv,
+    sv_gu, sv_pj, sv_dn, hidden_other, dn_other, own_sem, send_sem, recv_sem, side_send, side_recv,
 ):
     f32, bf16 = jnp.float32, jnp.bfloat16
     xs, ys, zs, near, other, tp = place()
@@ -275,6 +317,7 @@
             pj[zl, y, x] = pj_f32[...].astype(bf16)
             own[6].wait()
             dn[zl, y, x] = dn_f32[...].astype(bf16)
+            pass_on((0, 0, 0), 10)
 
     def part(c, at):
         name, i, width = WHERE[c]
@@ -331,7 +374,20 @@
     recv_rows = [to_other(rows.at[pl.ds(yours, 512)], rows.at[pl.ds(yours, 512)], i) for i in (0, 3)]
     send_sums = [to_other(psend, precv, i) for i in (1, 4)]
     send_square = to_other(square.at[pl.ds(yours, 512)], sqrecv, 2)
+    last_lanes = slice(1280, 1408)
+    send_hidden = to_other(hidden.at[pl.ds(yours, 512), last_lanes], hidden_other, 5)
+    last_chunk = CHUNK_OF[LAST]
+    arrived_last = []
     seen = set()
+
+    def pass_on(at, i):
+        z, y, x = at
+        z = slice(None) if z is None else int(z[-1]) if isinstance(z, str) else zs[z]
+        y = slice(None) if y is None else ys[y]
+        x = slice(None) if x is None else xs[x]
+        copy = to_other(part(last_chunk, at), dn_other.at[z, y, x], 6 + i)
+        copy.start()
+        arrived_last.append(copy)
 
     def block_norm():
         own[7].wait()
@@ -436,6 +492,8 @@
         before = jnp.zeros((8, 256), f32)
         for i in range(1024 // ROWS):
             before = body(i, before)
+        if k == 10:
+            send_hidden.start()
 
     def block_down(j):
         first, count = DOWN[j]
@@ -450,56 +508,82 @@
             for n in range(8):
                 store(n, slice(n * 256, n * 256 + 256), pl.ds(start, count), product(start, count, n))
 
-        if j < len(DOWN) - 1:
-
-            def store(n, cols, at, value):
-                acc[at, cols] = value if j == 0 else acc[at, cols] + value
-
-            sweep(0, 1024, store)
-            return
+        def store(n, cols, at, value):
+            acc[at, cols] = value if j == 0 else acc[at, cols] + value
+
+        sweep(0, 1024, store)
+
+
+    def block_give():
         send_sums[0].wait_send()
 
-        def give(n, cols, at, value):
-            psend[:, cols] = ((acc[at, cols] + value) * sv_dn[n]).astype(bf16)
-
-        sweep(yours, 512, give)
+        @pl.loop(0, 512, step=64)
+        def _(r):
+            at, there = pl.ds(pl.multiple_of(r, 64), 64), pl.ds(pl.multiple_of(yours + r, 64), 64)
+            for n in range(8):
+                cols = slice(256 * n, 256 * n + 256)
+                psend[at, cols] = (acc[there, cols] * sv_dn[n]).astype(bf16)
+
         send_sums[1].start()
 
-        def keep(n, cols, at, value):
-            acc[at, cols] = (acc[at, cols] + value) * sv_dn[n]
-
-        sweep(mine, 512, keep)
-
-    def block_last():
+    def block_base():
         send_sums[1].wait_recv()
-        for q in range(4):
-
-            @pl.loop(0, 128, step=64)
-            def _(r):
-                at = pl.ds(pl.multiple_of(q * 128 + r, 64), 64)
-                there = pl.ds(pl.multiple_of(mine + q * 128 + r, 64), 64)
-                summed = acc[there, :] + precv[at, :].astype(f32)
-                out[at, :] = (tok[at, :].astype(f32) + summed).astype(bf16)
+
+        @pl.loop(0, 512, step=64)
+        def _(r):
+            at, there = pl.ds(pl.multiple_of(r, 64), 64), pl.ds(pl.multiple_of(mine + r, 64), 64)
+            for n in range(8):
+                cols = slice(256 * n, 256 * n + 256)
+                summed = acc[there, cols] * sv_dn[n] + precv[at, cols].astype(f32)
+                acc[there, cols] = tok[at, cols].astype(f32) + summed
+
+    def block_final():
+        send_hidden.wait_recv()
+        for copy in arrived_last:
+            copy.wait_recv()
+        at = pl.ds(mine, 512)
+        left = jnp.concatenate([hidden[at, last_lanes], hidden_other[...]], axis=1)
+        for n in range(8):
+            cols = slice(256 * n, 256 * n + 256)
+            weights = [dn[n // 4, n % 4, :, :, last_lanes].reshape(256, 128), dn_other[n // 4, n % 4].reshape(256, 128)]
+            value = dot_nt(left, jnp.concatenate(weights, axis=1)) * sv_dn[n]
+            out[:, cols] = (acc[at, cols] + value).astype(bf16)
 
     blocks = {
         "cast": block_cast,
         "norm": block_norm, "scales": block_scales, "mix": block_mix, "conv": block_conv, "proj": block_proj,
-        "first": block_first, "gu": block_gu, "down": block_down, "last": block_last,
+        "first": block_first, "gu": block_gu, "down": block_down, "give": block_give, "base": block_base,
+        "final": block_final,
     }
-    for op in ops:
+    gone = set()
+
+    def sent_by(end):
+        for c, (kind, _, _) in enumerate(CHUNKS):
+            entries = range(len(TREES[kind]))
+            if c not in gone and all(("send", c, m) in ops[:end] for m in entries):
+                gone.add(c)
+                for m in entries:
+                    copy_of(c, m, False).wait_send()
+
+    for step, op in enumerate(ops):
         if op[0] == "send":
             copy_of(op[1], op[2], False).start()
         elif op[0] == "wait":
             copy_of(op[1], op[2], True).wait_recv()
+            if op[1] == last_chunk:
+                pass_on(carried(*CHUNKS[last_chunk][:1], op[2], CHUNKS[last_chunk][1], True), op[2])
         else:
             name, *index = names[op[1]]
+            if name == "base":
+                sent_by(step - 30)
             blocks[name](*index)
-    for c, (kind, turn, _) in enumerate(CHUNKS):
-        for m in range(len(TREES[kind])):
-            copy_of(c, m, False).wait_send()
+    sent_by(len(ops))
     send_square.wait_send()
     send_rows[1].wait_send()
     send_sums[1].wait_send()
+    send_hidden.wait_send()
+    for copy in arrived_last:
+        copy.wait_send()
 
 
 def mega(*args):
@@ -533,11 +617,13 @@
             pltpu.VMEM((11, 1, 256), f32),
             pltpu.VMEM((8, 1, 256), f32),
             pltpu.VMEM((8, 1, 256), f32),
+            pltpu.VMEM((512, 128), bf16),
+            pltpu.VMEM((2, 4, 4, 64, 128), bf16),
             dma((8,)),
             dma((len(CHUNKS),)),
             dma((len(CHUNKS), 10)),
-            dma((5,)),
-            dma((5,)),
+            dma((17,)),
+            dma((17,)),
         ],
         compiler_params=pltpu.CompilerParams(collective_id=0, has_side_effects=True, vmem_limit_bytes=58 * 1024 * 1024),
     )(*args)

time: 128 us -> 121 us (0.945)
  Pallas kernels: 127 us -> 120 us
    pallas_call x1, Pallas kernels: 126 us -> 119 us  [mega(): pl.pallas_call(lambda *refs: mega_kernel(ops, names, *refs), out_shape=pl...]
where the time goes in v2:
time: 121 us
  Pallas kernels  120 us (99%)
    pallas_call x1, Pallas kernels, mega(): pl.pallas_call(lambda *refs: mega_kernel(ops, names, *refs), out_shape=pl...  119 us

profile of v2, /device:TPU:1, one launch (start us, length us, event | category | flops | bytes accessed | tf_op | source)
XLA Modules:
  0.0 120.6 jit_solution(10519306955269727764)
XLA Ops:
  0.0 119.0 %shard_map.217.src = bf16[512,2048]{1,0:T(8,128)(2,1)S(1)} custom-call(bf16[512,2048]{1,0:T(8,128)(2,1)} %bitcast.4, f32[64,512]{1,0:T(8,128)} %refs_1_.1, f32[64,512]{1,0:T(8,128)} %refs_2_.1, f32[64,512]{1,0:T(8,128)} %refs_3_.1, f32[64,1408]{1,0:T(8,128)} %refs_4_.1, f32[64,1408]{1,0:T(8,128)} %refs_5_.1, f32[64,512]{1,0:T(8,128)} %bitcast.6, ...), custom_call_target="tpu_custom_call" | custom-call | tf_op jit(solution)/shard_map/pallas_call | solution.py:595
  119.1 1.3 %shard_map.218 = bf16[512,2048]{1,0:T(8,128)(2,1)} custom-call(bf16[512,2048]{1,0:T(8,128)(2,1)S(1)} %shard_map.217.src), custom_call_target="tpu_custom_call" | custom-call | tf_op jit(solution)/shard_map/pallas_call | solution.py:643

commit v3 on v2

--- a/solution.py
+++ b/solution.py
@@ -33,6 +33,21 @@
         ((4,), "x+", 4),
         ((5,), "x-", 4),
     ),
+    "E": (
+        ((), "x+", 1),
+        ((), "x-", 1),
+        ("s01", "xs", 1),
+        ((0, 1, 2), "y+", 4),
+        ((0, 1, 2), "y-", 4),
+        ((), "zs", 1),
+        ((0,), "zs", 1),
+        ((1,), "zs", 1),
+        ((2,), "zs", 1),
+        ("s34", "ys", 4),
+        ("s34", "zo", 4),
+        ("o34", "zo", 4),
+        ((9,), "zs", 4),
+    ),
     "C": (
         ((), "zs", 1),
         ((0,), "x+", 2),
@@ -60,35 +75,35 @@
     return name[0], sign
 
 
-RATE, HOP, AHEAD = 46.0, 2.2, 2.5
+RATE, HOP, AHEAD = 46.0, 2.2, 3
 ORDER = (
-    ("mix", 5, "A", 1),
-    ("gu", 10, "D", 1),
-    ("mix", 0, "A", -1),
-    ("mix", 2, "A", 1),
-    ("mix", 1, "D", 1),
-    ("mix", 4, "D", -1),
+    ("mix", 0, "A", 1),
+    ("mix", 2, "D", 1),
+    ("mix", 3, "E", 1),
+    ("mix", 5, "A", -1),
+    ("mix", 1, "E", -1),
+    ("gu", 1, "D", -1),
+    ("pj", 0, "D", -1),
+    ("mix", 4, "D", 1),
+    ("gu", 2, "E", 1),
     ("gu", 8, "A", -1),
-    ("pj", 1, "D", -1),
-    ("mix", 3, "A", 1),
-    ("pj", 0, "A", 1),
-    ("gu", 6, "A", 1),
-    ("gu", 2, "A", -1),
-    ("gu", 3, "A", -1),
-    ("dn", 0, "D", -1),
-    ("gu", 1, "D", 1),
-    ("gu", 0, "A", 1),
-    ("dn", 1, "A", -1),
-    ("gu", 4, "D", 1),
-    ("gu", 9, "A", 1),
-    ("gu", 5, "A", -1),
+    ("pj", 1, "A", -1),
     ("gu", 7, "D", 1),
     ("dn", 3, "A", 1),
+    ("gu", 0, "A", -1),
+    ("gu", 4, "D", 1),
+    ("gu", 3, "E", 1),
+    ("gu", 9, "D", -1),
+    ("dn", 0, "D", 1),
+    ("dn", 1, "A", -1),
+    ("gu", 5, "A", -1),
+    ("gu", 6, "A", -1),
+    ("dn", 2, "E", 1),
+    ("dn", 5, "D", -1),
+    ("gu", 10, "D", 1),
     ("dn", 4, "A", -1),
-    ("dn", 2, "D", -1),
-    ("dn", 5, "A", 1),
 )
-LEAD = {("A", 6): 1.0, ("C", 4): 12, ("D", 2): 0.5, ("D", 3): 9.0, ("D", 1): 6.0, ("D", 5): 3.5, ("D", 6): 10, ("A", 0): 0.5, ("D", 7): 8, ("D", 0): 4.0, ("A", 7): 1.5, ("C", 1): 5.0, ("A", 1): -3, ("A", 9): 3.0, ("A", 4): 1.0, ("A", 2): 9.0, ("A", 3): 0.5, ("C", 0): 1.5, ("D", 4): 6.0, ("C", 5): 9.5, ("C", 7): 8.0, ("C", 3): 1.5, ("A", 5): 1, ("C", 2): 8.0, ("A", 8): -0.5}
+LEAD = {("A", 6): 12, ("C", 4): 9, ("D", 2): 1.0, ("D", 3): 7.5, ("D", 1): 12, ("D", 5): 1.0, ("D", 6): 1.5, ("D", 7): 9.5, ("D", 0): 12, ("A", 7): 1.5, ("C", 1): 5.5, ("C", 6): 4.0, ("A", 1): 2.0, ("A", 9): 12, ("A", 4): 3.5, ("A", 2): 7.0, ("A", 3): 0.5, ("C", 0): 8.5, ("D", 4): -3, ("C", 5): 6, ("C", 7): 4.5, ("C", 3): 9, ("A", 5): 11.5, ("C", 2): 2.5, ("A", 8): 10, ("E", 7): 11.5, ("E", 10): 7.5, ("E", 8): 1, ("E", 0): -3, ("E", 2): -0.5, ("E", 9): -1.5, ("E", 3): 7.5, ("E", 5): 4.5, ("E", 4): -2.0, ("E", 1): -3, ("E", 12): 10, ("E", 6): 9.0}
 
 
 def plan(chunks, comps, own_after, rate=RATE, hop=HOP, issue=0.04, ahead=AHEAD):
@@ -162,7 +177,8 @@
 CHUNKS, WHERE = list_of_chunks()
 CHUNK_OF = {(name, i): c for c, (name, i, _) in enumerate(WHERE)}
 ROWS = 256
-DOWN = ((0, 2), (2, 2), (4, 1))
+DOWN = ((0, 2), (2, 2))
+PASSED = 4
 
 
 def list_of_blocks():
@@ -190,9 +206,10 @@
         units = range(first, first + count)
         before = [(("gu", k), 0.0) for u in units for k in (2 * u, 2 * u + 1)] + [(("down", j - 1), 0.0)] * (j > 0)
         add(("down", j), 0.1 + 1.15 * count, [("dn", u) for u in units], before)
-    add(("give",), 0.5, [], [(("down", len(DOWN) - 1), 0.0), (("gu", 10), 0.0)])
+    add(("give",), 0.5, [], [(("down", len(DOWN) - 1), 0.0)])
     add(("base",), 1.3, [], [(("give",), 4.2)])
-    add(("final",), 2.2, [LAST], [(("base",), 0.0)])
+    add(("near", 4), 1.3, [("dn", 4)], [(("base",), 0.0), (("gu", 8), 2.0), (("gu", 9), 2.0)])
+    add(("near", 5), 1.5, [("dn", 5)], [(("near", 4), 0.0), (("gu", 10), 2.0)])
     own_after = {}
     for (name, _), c in CHUNK_OF.items():
         if name in ("gu", "pj", "dn"):
@@ -240,6 +257,21 @@
             ("plane0", None, -1),
             ("plane1", None, 1),
         ),
+        "E": (
+            (0, 0, 0),
+            (0, 0, 0),
+            (0, 0, -turn),
+            (0, 0, None),
+            (0, 0, None),
+            (0, 0, 0),
+            (0, 0, -1),
+            (0, 0, 1),
+            (0, 0, 2),
+            (0, -turn, None),
+            (0, -turn, None),
+            (0, turn, None),
+            (0, 2, None),
+        ),
         "C": (
             (0, 0, 0),
             (None, 0, 0),
@@ -270,11 +302,19 @@
 
 
 def mega_kernel(
-    ops, names, tokens, in_w, val_w, out_w, gate_w, up_w, pj_w, dn_w, in_s, val_s, out_s, gate_s, up_s, pj_s, dn_s, mix_gain,
-    ffn_gain, mix_taps, conv_gain, gate_taps, up_taps, gate_bias, up_bias, out, mix, pj, gu, dn, sc, tok, rows, gates, conv, square, acc, hidden, psend, precv, sqrecv, sv_mix,
+    ops, names, tokens, in_w, val_w, out_w, gate_w, up_w, pj_w, dn_w, *rest,
+):
+    small_in, out, small = rest[:15], rest[15], rest[16:31]
+    run_kernel(ops, names, tokens, in_w, val_w, out_w, gate_w, up_w, pj_w, dn_w, small_in, small, out, *rest[31:])
+
+
+def run_kernel(
+    ops, names, tokens, in_w, val_w, out_w, gate_w, up_w, pj_w, dn_w, small_in, small, out, mix, pj, gu, dn, sc, tok, rows, gates, conv, square, acc, hidden, psend, precv, sqrecv, sv_mix,
     sv_gu, sv_pj, sv_dn, hidden_other, dn_other, own_sem, send_sem, recv_sem, side_send, side_recv,
 ):
     f32, bf16 = jnp.float32, jnp.bfloat16
+    (in_s, val_s, out_s, gate_s, up_s, pj_s, dn_s, mix_gain, ffn_gain, mix_taps, conv_gain, gate_taps, up_taps, gate_bias,
+     up_bias) = small
     xs, ys, zs, near, other, tp = place()
     bufs = {"mix": mix, "pj": pj, "gu": gu, "dn": dn, "sc": sc}
     x, y, zl = xs[0], ys[0], zs[0]
@@ -292,12 +332,15 @@
             )
         )
     ]
-    for copy in own:
+    small_copies = [pltpu.make_async_copy(src, dst, own_sem.at[8 + i]) for i, (src, dst) in enumerate(zip(small_in, small))]
+    for copy in own[:3] + small_copies[:7] + own[3:] + small_copies[7:]:
         copy.start()
     barrier = pltpu.get_barrier_semaphore()
     for device in [*near.values(), other]:
         pl.semaphore_signal(barrier, inc=1, device_id=device, device_id_type=MESH)
     sc[zl, y, x] = jnp.zeros((8, 128), f32)
+    for copy in small_copies[:7]:
+        copy.wait()
     for i, ref in enumerate((in_s, val_s, out_s, gate_s, up_s, pj_s, dn_s)):
         sc[zl, y, x, i : i + 1, : ref.shape[0]] = ref[...].reshape(1, -1)
     for i in range(3):
@@ -317,7 +360,8 @@
             pj[zl, y, x] = pj_f32[...].astype(bf16)
             own[6].wait()
             dn[zl, y, x] = dn_f32[...].astype(bf16)
-            pass_on((0, 0, 0), 10)
+            for unit in passed:
+                pass_on(unit, (0, 0, 0), 13)
 
     def part(c, at):
         name, i, width = WHERE[c]
@@ -374,23 +418,30 @@
     recv_rows = [to_other(rows.at[pl.ds(yours, 512)], rows.at[pl.ds(yours, 512)], i) for i in (0, 3)]
     send_sums = [to_other(psend, precv, i) for i in (1, 4)]
     send_square = to_other(square.at[pl.ds(yours, 512)], sqrecv, 2)
-    last_lanes = slice(1280, 1408)
-    send_hidden = to_other(hidden.at[pl.ds(yours, 512), last_lanes], hidden_other, 5)
-    last_chunk = CHUNK_OF[LAST]
-    arrived_last = []
+    def lanes_of(unit):
+        return slice(UNIT * unit, min(UNIT * unit + UNIT, 1408)), slice(UNIT * (unit - PASSED), min(UNIT * unit + UNIT, 1408) - UNIT * PASSED)
+
+    send_hidden = {}
+    for unit in (4, 5):
+        here, there = lanes_of(unit)
+        send_hidden[unit] = to_other(hidden.at[pl.ds(yours, 512), here], hidden_other.at[:, there], 1 + unit)
+    passed = {4: [], 5: []}
     seen = set()
 
-    def pass_on(at, i):
+    def pass_on(unit, at, i):
         z, y, x = at
         z = slice(None) if z is None else int(z[-1]) if isinstance(z, str) else zs[z]
         y = slice(None) if y is None else ys[y]
         x = slice(None) if x is None else xs[x]
-        copy = to_other(part(last_chunk, at), dn_other.at[z, y, x], 6 + i)
+        ref = dn_other.at[z, y, x, :, lanes_of(unit)[1]]
+        copy = to_other(part(CHUNK_OF["dn", unit], at), ref, 7 + 14 * (unit - PASSED) + i)
         copy.start()
-        arrived_last.append(copy)
+        passed[unit].append(copy)
 
     def block_norm():
         own[7].wait()
+        for copy in small_copies[7:]:
+            copy.wait()
 
         @pl.loop(0, 512, step=64)
         def _(r):
@@ -492,8 +543,11 @@
         before = jnp.zeros((8, 256), f32)
         for i in range(1024 // ROWS):
             before = body(i, before)
+        seen.add(k)
         if k == 10:
-            send_hidden.start()
+            send_hidden[5].start()
+        elif k in (8, 9) and {8, 9} <= seen:
+            send_hidden[4].start()
 
     def block_down(j):
         first, count = DOWN[j]
@@ -537,23 +591,28 @@
                 summed = acc[there, cols] * sv_dn[n] + precv[at, cols].astype(f32)
                 acc[there, cols] = tok[at, cols].astype(f32) + summed
 
-    def block_final():
-        send_hidden.wait_recv()
-        for copy in arrived_last:
+    def block_near(unit):
+        send_hidden[unit].wait_recv()
+        for copy in passed[unit]:
             copy.wait_recv()
+        here, there = lanes_of(unit)
+        width = here.stop - here.start
         at = pl.ds(mine, 512)
-        left = jnp.concatenate([hidden[at, last_lanes], hidden_other[...]], axis=1)
+        left = jnp.concatenate([hidden[at, here], hidden_other[:, there]], axis=1)
         for n in range(8):
             cols = slice(256 * n, 256 * n + 256)
-            weights = [dn[n // 4, n % 4, :, :, last_lanes].reshape(256, 128), dn_other[n // 4, n % 4].reshape(256, 128)]
-            value = dot_nt(left, jnp.concatenate(weights, axis=1)) * sv_dn[n]
-            out[:, cols] = (acc[at, cols] + value).astype(bf16)
+            weights = [ref[n // 4, n % 4, :, :, lanes].reshape(256, width) for ref, lanes in ((dn, here), (dn_other, there))]
+            value = acc[at, cols] + dot_nt(left, jnp.concatenate(weights, axis=1)) * sv_dn[n]
+            if unit == 5:
+                out[:, cols] = value.astype(bf16)
+            else:
+                acc[at, cols] = value
 
     blocks = {
         "cast": block_cast,
         "norm": block_norm, "scales": block_scales, "mix": block_mix, "conv": block_conv, "proj": block_proj,
         "first": block_first, "gu": block_gu, "down": block_down, "give": block_give, "base": block_base,
-        "final": block_final,
+        "near": block_near,
     }
     gone = set()
 
@@ -570,8 +629,9 @@
             copy_of(op[1], op[2], False).start()
         elif op[0] == "wait":
             copy_of(op[1], op[2], True).wait_recv()
-            if op[1] == last_chunk:
-                pass_on(carried(*CHUNKS[last_chunk][:1], op[2], CHUNKS[last_chunk][1], True), op[2])
+            name, unit, _ = WHERE[op[1]]
+            if name == "dn" and unit in passed:
+                pass_on(unit, carried(CHUNKS[op[1]][0], op[2], CHUNKS[op[1]][1], True), op[2])
         else:
             name, *index = names[op[1]]
             if name == "base":
@@ -581,9 +641,9 @@
     send_square.wait_send()
     send_rows[1].wait_send()
     send_sums[1].wait_send()
-    send_hidden.wait_send()
-    for copy in arrived_last:
-        copy.wait_send()
+    for unit in passed:
+        for copy in [send_hidden[unit], *passed[unit]]:
+            copy.wait_send()
 
 
 def mega(*args):
@@ -595,9 +655,9 @@
     return pl.pallas_call(
         lambda *refs: mega_kernel(ops, names, *refs),
         out_shape=pltpu.VMEM((512, 2048), bf16),
-        in_specs=[hbm] * 8 + [vmem] * 15,
+        in_specs=[hbm] * 23,
         out_specs=vmem,
-        scratch_shapes=[
+        scratch_shapes=[pltpu.VMEM(a.shape, f32) for a in args[8:]] + [
             pltpu.VMEM((6, 2, 4, 4, 64, 256), bf16),
             pltpu.VMEM((2, 4, 4, 64, 512), bf16),
             pltpu.VMEM((11, 2, 4, 4, 64, 256), bf16),
@@ -617,13 +677,13 @@
             pltpu.VMEM((11, 1, 256), f32),
             pltpu.VMEM((8, 1, 256), f32),
             pltpu.VMEM((8, 1, 256), f32),
-            pltpu.VMEM((512, 128), bf16),
-            pltpu.VMEM((2, 4, 4, 64, 128), bf16),
-            dma((8,)),
+            pltpu.VMEM((512, 384), bf16),
+            pltpu.VMEM((2, 4, 4, 64, 384), bf16),
+            dma((23,)),
             dma((len(CHUNKS),)),
-            dma((len(CHUNKS), 10)),
-            dma((17,)),
-            dma((17,)),
+            dma((len(CHUNKS), 13)),
+            dma((35,)),
+            dma((35,)),
         ],
         compiler_params=pltpu.CompilerParams(collective_id=0, has_side_effects=True, vmem_limit_bytes=58 * 1024 * 1024),
     )(*args)

time: 121 us -> 121 us (level)
  no operation moved by 1% of the time
where the time goes in v3:
time: 121 us
  Pallas kernels  121 us (100%)
    pallas_call x1, Pallas kernels, mega(): pl.pallas_call(lambda *refs: mega_kernel(ops, names, *refs), out_shape=pl...  120 us

profile of v3, /device:TPU:1, one launch (start us, length us, event | category | flops | bytes accessed | tf_op | source)
XLA Modules:
  0.0 121.3 jit_solution(475027216951014556)
XLA Ops:
  0.0 119.8 %shard_map.217.src = bf16[512,2048]{1,0:T(8,128)(2,1)S(1)} custom-call(bf16[512,2048]{1,0:T(8,128)(2,1)} %bitcast.4, f32[64,512]{1,0:T(8,128)} %refs_1_.1, f32[64,512]{1,0:T(8,128)} %refs_2_.1, f32[64,512]{1,0:T(8,128)} %refs_3_.1, f32[64,1408]{1,0:T(8,128)} %refs_4_.1, f32[64,1408]{1,0:T(8,128)} %refs_5_.1, f32[64,512]{1,0:T(8,128)} %bitcast.6, ...), custom_call_target="tpu_custom_call" | custom-call | tf_op jit(solution)/shard_map/pallas_call | solution.py:655
  119.8 1.3 %shard_map.218 = bf16[512,2048]{1,0:T(8,128)(2,1)} custom-call(bf16[512,2048]{1,0:T(8,128)(2,1)S(1)} %shard_map.217.src), custom_call_target="tpu_custom_call" | custom-call | tf_op jit(solution)/shard_map/pallas_call | solution.py:703

commit v4 on v3

--- a/solution.py
+++ b/solution.py
@@ -75,35 +75,35 @@
     return name[0], sign
 
 
-RATE, HOP, AHEAD = 46.0, 2.2, 3
+RATE, HOP, AHEAD = 46.5, 2.2, 1.5
 ORDER = (
+    ("mix", 4, "D", -1),
+    ("pj", 1, "D", -1),
     ("mix", 0, "A", 1),
+    ("gu", 8, "E", -1),
+    ("dn", 3, "A", 1),
     ("mix", 2, "D", 1),
-    ("mix", 3, "E", 1),
+    ("mix", 3, "A", 1),
+    ("mix", 1, "E", -1),
     ("mix", 5, "A", -1),
-    ("mix", 1, "E", -1),
-    ("gu", 1, "D", -1),
-    ("pj", 0, "D", -1),
-    ("mix", 4, "D", 1),
-    ("gu", 2, "E", 1),
-    ("gu", 8, "A", -1),
-    ("pj", 1, "A", -1),
+    ("pj", 0, "D", 1),
+    ("gu", 5, "A", -1),
+    ("gu", 1, "D", 1),
+    ("gu", 4, "A", 1),
     ("gu", 7, "D", 1),
-    ("dn", 3, "A", 1),
+    ("gu", 3, "E", -1),
+    ("gu", 2, "A", -1),
+    ("gu", 9, "D", -1),
+    ("dn", 1, "E", 1),
+    ("gu", 6, "E", -1),
+    ("dn", 0, "D", 1),
     ("gu", 0, "A", -1),
-    ("gu", 4, "D", 1),
-    ("gu", 3, "E", 1),
-    ("gu", 9, "D", -1),
-    ("dn", 0, "D", 1),
-    ("dn", 1, "A", -1),
-    ("gu", 5, "A", -1),
-    ("gu", 6, "A", -1),
     ("dn", 2, "E", 1),
+    ("gu", 10, "E", 1),
     ("dn", 5, "D", -1),
-    ("gu", 10, "D", 1),
-    ("dn", 4, "A", -1),
+    ("dn", 4, "E", 1),
 )
-LEAD = {("A", 6): 12, ("C", 4): 9, ("D", 2): 1.0, ("D", 3): 7.5, ("D", 1): 12, ("D", 5): 1.0, ("D", 6): 1.5, ("D", 7): 9.5, ("D", 0): 12, ("A", 7): 1.5, ("C", 1): 5.5, ("C", 6): 4.0, ("A", 1): 2.0, ("A", 9): 12, ("A", 4): 3.5, ("A", 2): 7.0, ("A", 3): 0.5, ("C", 0): 8.5, ("D", 4): -3, ("C", 5): 6, ("C", 7): 4.5, ("C", 3): 9, ("A", 5): 11.5, ("C", 2): 2.5, ("A", 8): 10, ("E", 7): 11.5, ("E", 10): 7.5, ("E", 8): 1, ("E", 0): -3, ("E", 2): -0.5, ("E", 9): -1.5, ("E", 3): 7.5, ("E", 5): 4.5, ("E", 4): -2.0, ("E", 1): -3, ("E", 12): 10, ("E", 6): 9.0}
+LEAD = {("A", 6): 7.5, ("C", 4): 2.5, ("D", 2): 0.5, ("D", 3): 8.0, ("D", 1): 9.5, ("D", 5): 3, ("D", 6): 12, ("A", 0): 2.5, ("D", 7): 10.0, ("D", 0): 4.0, ("A", 7): 12, ("C", 1): 6.0, ("C", 6): 0.5, ("A", 1): -1.0, ("A", 9): -2.5, ("A", 4): 1.5, ("A", 2): 12, ("A", 3): 6.0, ("C", 0): 7.5, ("D", 4): 6.0, ("C", 5): 8.5, ("C", 7): -2.0, ("C", 3): -2.5, ("A", 5): 1, ("C", 2): 5.0, ("A", 8): 12, ("E", 7): 8, ("E", 11): -2, ("E", 8): -1.5, ("E", 0): -0.5, ("E", 2): -2.5, ("E", 9): 3.0, ("E", 3): 12, ("E", 5): 0.5, ("E", 4): -3, ("E", 1): -3, ("E", 12): 2.5, ("E", 6): 12}
 
 
 def plan(chunks, comps, own_after, rate=RATE, hop=HOP, issue=0.04, ahead=AHEAD):
@@ -191,25 +191,25 @@
 
     add(("cast", "gu"), 0.5)
     add(("cast", "rest"), 0.4)
-    add(("norm",), 1.5)
-    add(("scales",), 1.0, [("sc", 0)])
+    add(("norm",), 1.3)
+    add(("scales",), 0.3, [("sc", 0)])
     for k in range(6):
-        add(("mix", k), 1.05, [("mix", k)], [(("norm",), 4.0), (("scales",), 0.0)])
+        add(("mix", k), 1.25, [("mix", k)], [(("norm",), 4.0), (("scales",), 0.0)])
     for g in range(2):
-        add(("conv", g), 1.0, [], [(("mix", 3 * g + i), 0.0) for i in range(3)] + [(("conv", 0), 0.0)] * g)
-    add(("proj", 0), 0.8, [("pj", 0), ("pj", 1)], [(("conv", 0), 0.0), (("conv", 1), 0.0)])
-    add(("proj", 1), 0.8, [], [(("proj", 0), 0.0)])
-    add(("first",), 2.0, [], [(("proj", 1), 3.2)])
+        add(("conv", g), 1.3, [], [(("mix", 3 * g + i), 0.0) for i in range(3)] + [(("conv", 0), 0.0)] * g)
+    add(("proj", 0), 1.3, [("pj", 0), ("pj", 1)], [(("conv", 0), 0.0), (("conv", 1), 0.0)])
+    add(("proj", 1), 1.3, [], [(("proj", 0), 0.0)])
+    add(("first",), 2.8, [], [(("proj", 1), 0.0), (("proj", 0), 2.0)])
     for k in range(11):
-        add(("gu", k), 1.45, [("gu", k)], [(("first",), 4.0)])
+        add(("gu", k), 1.75, [("gu", k)], [(("first",), 2.2)])
     for j, (first, count) in enumerate(DOWN):
         units = range(first, first + count)
         before = [(("gu", k), 0.0) for u in units for k in (2 * u, 2 * u + 1)] + [(("down", j - 1), 0.0)] * (j > 0)
-        add(("down", j), 0.1 + 1.15 * count, [("dn", u) for u in units], before)
-    add(("give",), 0.5, [], [(("down", len(DOWN) - 1), 0.0)])
-    add(("base",), 1.3, [], [(("give",), 4.2)])
-    add(("near", 4), 1.3, [("dn", 4)], [(("base",), 0.0), (("gu", 8), 2.0), (("gu", 9), 2.0)])
-    add(("near", 5), 1.5, [("dn", 5)], [(("near", 4), 0.0), (("gu", 10), 2.0)])
+        add(("down", j), 2.4, [("dn", u) for u in units], before)
+    add(("give",), 0.3, [], [(("down", len(DOWN) - 1), 0.0)])
+    add(("base",), 0.9, [], [(("give",), 4.2)])
+    add(("near", 4), 1.7, [("dn", 4)], [(("base",), 0.0), (("gu", 8), 2.0), (("gu", 9), 2.0)])
+    add(("near", 5), 1.9, [("dn", 5)], [(("near", 4), 0.0), (("gu", 10), 2.0)])
     own_after = {}
     for (name, _), c in CHUNK_OF.items():
         if name in ("gu", "pj", "dn"):
@@ -414,9 +414,14 @@
             total = jnp.where((lane >= at) & (lane < at + width), line, total)
         return total
 
-    send_rows = [to_other(rows.at[pl.ds(mine, 512)], rows.at[pl.ds(mine, 512)], i) for i in (0, 3)]
-    recv_rows = [to_other(rows.at[pl.ds(yours, 512)], rows.at[pl.ds(yours, 512)], i) for i in (0, 3)]
-    send_sums = [to_other(psend, precv, i) for i in (1, 4)]
+    def rows_copy(to_send, first, count, i):
+        at = pl.ds((mine if to_send else yours) + first, count)
+        return to_other(rows.at[at], rows.at[at], i)
+
+    send_rows, recv_rows = (rows_copy(b, 0, 512, 0) for b in (True, False))
+    send_again, recv_again = ([rows_copy(b, 128 * q, 128, 35 + q) for q in range(4)] for b in (True, False))
+    send_parts = [to_other(psend.at[pl.ds(256 * q, 256)], precv.at[pl.ds(256 * q, 256)], (1, 3)[q]) for q in range(2)]
+    send_sums = to_other(psend, precv, 4)
     send_square = to_other(square.at[pl.ds(yours, 512)], sqrecv, 2)
     def lanes_of(unit):
         return slice(UNIT * unit, min(UNIT * unit + UNIT, 1408)), slice(UNIT * (unit - PASSED), min(UNIT * unit + UNIT, 1408) - UNIT * PASSED)
@@ -448,7 +453,7 @@
             at = pl.multiple_of(r, 64)
             rows[pl.ds(mine + at, 64), :] = normed(tok[pl.ds(at, 64), :].astype(f32), mix_gain)
 
-        send_rows[0].start()
+        send_rows.start()
 
     def block_scales():
         for k in range(6):
@@ -464,7 +469,7 @@
     def block_mix(k):
         if "rows" not in seen:
             seen.add("rows")
-            recv_rows[0].wait_recv()
+            recv_rows.wait_recv()
 
         for r in range(0, 1024, ROWS):
             at = pl.ds(r, ROWS)
@@ -491,41 +496,44 @@
             send_square.start()
 
     def block_proj(half):
-        start = yours if half == 0 else mine
-
-        for n in range(8):
-            weight = pj[n // 4, n % 4].reshape(256, 512)
-            part_sum = dot_nt(conv[pl.ds(start, 512), :], weight) * sv_pj[n]
-            cols = slice(n * 256, n * 256 + 256)
+        for q in range(2):
+            here = pl.ds(256 * q, 256)
+            rows_at = pl.ds((yours if half == 0 else mine) + 256 * q, 256)
+            for n in range(8):
+                weight = pj[n // 4, n % 4].reshape(256, 512)
+                part_sum = dot_nt(conv[rows_at, :], weight) * sv_pj[n]
+                cols = slice(n * 256, n * 256 + 256)
+                if half == 0:
+                    psend[here, cols] = part_sum.astype(bf16)
+                else:
+                    acc[rows_at, cols] = part_sum
             if half == 0:
-                psend[:, cols] = part_sum.astype(bf16)
-            else:
-                acc[pl.ds(start, 512), cols] = part_sum
-
-        if half == 0:
-            send_sums[0].start()
+                send_parts[q].start()
 
     def block_first():
-        send_sums[0].wait_recv()
         send_square.wait_recv()
-        send_rows[0].wait_send()
-
-        @pl.loop(0, 512, step=64)
-        def _(r):
-            at = pl.ds(pl.multiple_of(r, 64), 64)
-            there = pl.ds(pl.multiple_of(mine + r, 64), 64)
-            squares = square[there, :1] + sqrecv[at, :1]
-            summed = (acc[there, :] + precv[at, :].astype(f32)) * lax.rsqrt(squares / 1024 + epsilon)
-            first = (tok[at, :].astype(f32) + summed).astype(bf16)
-            tok[at, :] = first
-            rows[there, :] = normed(first.astype(f32), ffn_gain)
-
-        send_rows[1].start()
+        send_rows.wait_send()
+        for q in range(4):
+            if q % 2 == 0:
+                send_parts[q // 2].wait_recv()
+
+            @pl.loop(128 * q, 128 * q + 128, step=64)
+            def _(r):
+                at = pl.ds(pl.multiple_of(r, 64), 64)
+                there = pl.ds(pl.multiple_of(mine + r, 64), 64)
+                squares = square[there, :1] + sqrecv[at, :1]
+                summed = (acc[there, :] + precv[at, :].astype(f32)) * lax.rsqrt(squares / 1024 + epsilon)
+                first = (tok[at, :].astype(f32) + summed).astype(bf16)
+                tok[at, :] = first
+                rows[there, :] = normed(first.astype(f32), ffn_gain)
+
+            send_again[q].start()
 
     def block_gu(k):
         if "rows2" not in seen:
             seen.add("rows2")
-            recv_rows[1].wait_recv()
+            for copy in recv_again:
+                copy.wait_recv()
         cols = slice(128 * k, 128 * k + 128)
 
         def body(i, before):
@@ -537,7 +545,8 @@
             for j, (taps, bias) in enumerate(((gate_taps, gate_bias), (up_taps, up_bias))):
                 half, t = slice(128 * j, 128 * j + 128), taps[:, cols]
                 acts.append(t[0:1] * two[:, half] + t[1:2] * one[:, half] + t[2:3] * pre[:, half] + bias[cols].reshape(1, 128))
-            hidden[at, cols] = (acts[0] / (1.0 + jnp.exp(-acts[0])) * acts[1]).astype(bf16)
+            half = 0.5 * acts[0]
+            hidden[at, cols] = ((half + half * jnp.tanh(half)) * acts[1]).astype(bf16)
             return pre[-8:]
 
         before = jnp.zeros((8, 256), f32)
@@ -569,7 +578,8 @@
 
 
     def block_give():
-        send_sums[0].wait_send()
+        for copy in send_parts:
+            copy.wait_send()
 
         @pl.loop(0, 512, step=64)
         def _(r):
@@ -578,10 +588,10 @@
                 cols = slice(256 * n, 256 * n + 256)
                 psend[at, cols] = (acc[there, cols] * sv_dn[n]).astype(bf16)
 
-        send_sums[1].start()
+        send_sums.start()
 
     def block_base():
-        send_sums[1].wait_recv()
+        send_sums.wait_recv()
 
         @pl.loop(0, 512, step=64)
         def _(r):
@@ -639,8 +649,9 @@
             blocks[name](*index)
     sent_by(len(ops))
     send_square.wait_send()
-    send_rows[1].wait_send()
-    send_sums[1].wait_send()
+    send_sums.wait_send()
+    for copy in send_again:
+        copy.wait_send()
     for unit in passed:
         for copy in [send_hidden[unit], *passed[unit]]:
             copy.wait_send()
@@ -682,8 +693,8 @@
             dma((23,)),
             dma((len(CHUNKS),)),
             dma((len(CHUNKS), 13)),
-            dma((35,)),
-            dma((35,)),
+            dma((39,)),
+            dma((39,)),
         ],
         compiler_params=pltpu.CompilerParams(collective_id=0, has_side_effects=True, vmem_limit_bytes=58 * 1024 * 1024),
     )(*args)

time: 121 us -> 119 us (0.983)
  Pallas kernels: 121 us -> 119 us
    pallas_call x1, Pallas kernels: 120 us -> 118 us  [mega(): pl.pallas_call(lambda *refs: mega_kernel(ops, names, *refs), out_shape=pl...]
where the time goes in v4:
time: 119 us
  Pallas kernels  119 us (100%)
    pallas_call x1, Pallas kernels, mega(): pl.pallas_call(lambda *refs: mega_kernel(ops, names, *refs), out_shape=pl...  118 us

profile of v4, /device:TPU:1, one launch (start us, length us, event | category | flops | bytes accessed | tf_op | source)
XLA Modules:
  0.0 119.2 jit_solution(9933355780627173967)
XLA Ops:
  0.0 117.7 %shard_map.217.src = bf16[512,2048]{1,0:T(8,128)(2,1)S(1)} custom-call(bf16[512,2048]{1,0:T(8,128)(2,1)} %bitcast.4, f32[64,512]{1,0:T(8,128)} %refs_1_.1, f32[64,512]{1,0:T(8,128)} %refs_2_.1, f32[64,512]{1,0:T(8,128)} %refs_3_.1, f32[64,1408]{1,0:T(8,128)} %refs_4_.1, f32[64,1408]{1,0:T(8,128)} %refs_5_.1, f32[64,512]{1,0:T(8,128)} %bitcast.6, ...), custom_call_target="tpu_custom_call" | custom-call | tf_op jit(solution)/shard_map/pallas_call | solution.py:666
  117.7 1.3 %shard_map.218 = bf16[512,2048]{1,0:T(8,128)(2,1)} custom-call(bf16[512,2048]{1,0:T(8,128)(2,1)S(1)} %shard_map.217.src), custom_call_target="tpu_custom_call" | custom-call | tf_op jit(solution)/shard_map/pallas_call | solution.py:714

commit v5 on v4

--- a/solution.py
+++ b/solution.py
@@ -59,6 +59,19 @@
         ((5,), "y-", 4),
     ),
 }
+
+
+ENDS = {
+    "A": ((5, 7, 8, 9), (1, None, None)),
+    "E": ((5, 6, 7, 8, 10, 11, 12), (1, None, None)),
+    "D": ((6, 7), (None, None, 2)),
+    "C": ((6, 7), (None, 2, None)),
+}
+
+
+def slot_of(kind, m):
+    ends = ENDS[kind][0]
+    return 0 if m in ends else 1 + [k for k in range(len(TREES[kind])) if k not in ends].index(m)
 
 
 def needs_of(kind, m, turn):
@@ -361,7 +374,7 @@
             own[6].wait()
             dn[zl, y, x] = dn_f32[...].astype(bf16)
             for unit in passed:
-                pass_on(unit, (0, 0, 0), 13)
+                pass_on(unit, (0, 0, 0))
 
     def part(c, at):
         name, i, width = WHERE[c]
@@ -376,14 +389,19 @@
             return ref.at[z, y, x]
         return ref.at[z, y, x, :, i * UNIT : i * UNIT + width]
 
+    def all_of(c, m):
+        kind, turn, _ = CHUNKS[c]
+        ends, region = ENDS[kind]
+        return region if m in ends else carried(kind, m, turn, True)
+
     def copy_of(c, m, arriving):
         kind, turn, _ = CHUNKS[c]
-        ref = part(c, carried(kind, m, turn, arriving))
+        ref = part(c, all_of(c, m) if arriving else carried(kind, m, turn, False))
         return pltpu.make_async_remote_copy(
             src_ref=ref,
             dst_ref=ref,
             send_sem=send_sem.at[c],
-            recv_sem=recv_sem.at[c, m],
+            recv_sem=recv_sem.at[c, slot_of(kind, m)],
             device_id=near[link_of(kind, m, turn)],
             device_id_type=MESH,
         )
@@ -419,7 +437,7 @@
         return to_other(rows.at[at], rows.at[at], i)
 
     send_rows, recv_rows = (rows_copy(b, 0, 512, 0) for b in (True, False))
-    send_again, recv_again = ([rows_copy(b, 128 * q, 128, 35 + q) for q in range(4)] for b in (True, False))
+    send_again, recv_again = ([rows_copy(b, 128 * q, 128, 9 + q) for q in range(4)] for b in (True, False))
     send_parts = [to_other(psend.at[pl.ds(256 * q, 256)], precv.at[pl.ds(256 * q, 256)], (1, 3)[q]) for q in range(2)]
     send_sums = to_other(psend, precv, 4)
     send_square = to_other(square.at[pl.ds(yours, 512)], sqrecv, 2)
@@ -430,18 +448,19 @@
     for unit in (4, 5):
         here, there = lanes_of(unit)
         send_hidden[unit] = to_other(hidden.at[pl.ds(yours, 512), here], hidden_other.at[:, there], 1 + unit)
-    passed = {4: [], 5: []}
+    passed = {}
+    for unit in (4, 5):
+        here, there = lanes_of(unit)
+        passed[unit] = to_other(dn.at[:, :, :, :, here], dn_other.at[:, :, :, :, there], 3 + unit)
     seen = set()
 
-    def pass_on(unit, at, i):
+    def pass_on(unit, at):
         z, y, x = at
         z = slice(None) if z is None else int(z[-1]) if isinstance(z, str) else zs[z]
         y = slice(None) if y is None else ys[y]
         x = slice(None) if x is None else xs[x]
         ref = dn_other.at[z, y, x, :, lanes_of(unit)[1]]
-        copy = to_other(part(CHUNK_OF["dn", unit], at), ref, 7 + 14 * (unit - PASSED) + i)
-        copy.start()
-        passed[unit].append(copy)
+        to_other(part(CHUNK_OF["dn", unit], at), ref, 3 + unit).start()
 
     def block_norm():
         own[7].wait()
@@ -603,8 +622,7 @@
 
     def block_near(unit):
         send_hidden[unit].wait_recv()
-        for copy in passed[unit]:
-            copy.wait_recv()
+        passed[unit].wait_recv()
         here, there = lanes_of(unit)
         width = here.stop - here.start
         at = pl.ds(mine, 512)
@@ -624,7 +642,7 @@
         "first": block_first, "gu": block_gu, "down": block_down, "give": block_give, "base": block_base,
         "near": block_near,
     }
-    gone = set()
+    gone, met = set(), set()
 
     def sent_by(end):
         for c, (kind, _, _) in enumerate(CHUNKS):
@@ -638,10 +656,14 @@
         if op[0] == "send":
             copy_of(op[1], op[2], False).start()
         elif op[0] == "wait":
-            copy_of(op[1], op[2], True).wait_recv()
-            name, unit, _ = WHERE[op[1]]
+            c, m = op[1:]
+            if (c, slot_of(CHUNKS[c][0], m)) in met:
+                continue
+            met.add((c, slot_of(CHUNKS[c][0], m)))
+            copy_of(c, m, True).wait_recv()
+            name, unit, _ = WHERE[c]
             if name == "dn" and unit in passed:
-                pass_on(unit, carried(CHUNKS[op[1]][0], op[2], CHUNKS[op[1]][1], True), op[2])
+                pass_on(unit, all_of(c, m))
         else:
             name, *index = names[op[1]]
             if name == "base":
@@ -653,8 +675,8 @@
     for copy in send_again:
         copy.wait_send()
     for unit in passed:
-        for copy in [send_hidden[unit], *passed[unit]]:
-            copy.wait_send()
+        send_hidden[unit].wait_send()
+        passed[unit].wait_send()
 
 
 def mega(*args):
@@ -692,9 +714,9 @@
             pltpu.VMEM((2, 4, 4, 64, 384), bf16),
             dma((23,)),
             dma((len(CHUNKS),)),
-            dma((len(CHUNKS), 13)),
-            dma((39,)),
-            dma((39,)),
+            dma((len(CHUNKS), 7)),
+            dma((13,)),
+            dma((13,)),
         ],
         compiler_params=pltpu.CompilerParams(collective_id=0, has_side_effects=True, vmem_limit_bytes=58 * 1024 * 1024),
     )(*args)

time: 119 us -> 117 us (0.983)
  Pallas kernels: 119 us -> 117 us
    pallas_call x1, Pallas kernels: 118 us -> 116 us  [mega(): pl.pallas_call(lambda *refs: mega_kernel(ops, names, *refs), out_shape=pl...]
where the time goes in v5:
time: 117 us
  Pallas kernels  117 us (100%)
    pallas_call x1, Pallas kernels, mega(): pl.pallas_call(lambda *refs: mega_kernel(ops, names, *refs), out_shape=pl...  116 us

profile of v5, /device:TPU:1, one launch (start us, length us, event | category | flops | bytes accessed | tf_op | source)
XLA Modules:
  0.0 117.2 jit_solution(2529730341133243107)
XLA Ops:
  0.0 115.7 %shard_map.217.src = bf16[512,2048]{1,0:T(8,128)(2,1)S(1)} custom-call(bf16[512,2048]{1,0:T(8,128)(2,1)} %bitcast.4, f32[64,512]{1,0:T(8,128)} %refs_1_.1, f32[64,512]{1,0:T(8,128)} %refs_2_.1, f32[64,512]{1,0:T(8,128)} %refs_3_.1, f32[64,1408]{1,0:T(8,128)} %refs_4_.1, f32[64,1408]{1,0:T(8,128)} %refs_5_.1, f32[64,512]{1,0:T(8,128)} %bitcast.6, ...), custom_call_target="tpu_custom_call" | custom-call | tf_op jit(solution)/shard_map/pallas_call | solution.py:688
  115.7 1.3 %shard_map.218 = bf16[512,2048]{1,0:T(8,128)(2,1)} custom-call(bf16[512,2048]{1,0:T(8,128)(2,1)S(1)} %shard_map.217.src), custom_call_target="tpu_custom_call" | custom-call | tf_op jit(solution)/shard_map/pallas_call | solution.py:736

commit v6 on v5

--- a/solution.py
+++ b/solution.py
@@ -221,7 +221,7 @@
         add(("down", j), 2.4, [("dn", u) for u in units], before)
     add(("give",), 0.3, [], [(("down", len(DOWN) - 1), 0.0)])
     add(("base",), 0.9, [], [(("give",), 4.2)])
-    add(("near", 4), 1.7, [("dn", 4)], [(("base",), 0.0), (("gu", 8), 2.0), (("gu", 9), 2.0)])
+    add(("near", 4), 1.7, [("dn", 4), ("dn", 5)], [(("base",), 0.0), (("gu", 8), 2.0), (("gu", 9), 2.0)])
     add(("near", 5), 1.9, [("dn", 5)], [(("near", 4), 0.0), (("gu", 10), 2.0)])
     own_after = {}
     for (name, _), c in CHUNK_OF.items():
@@ -621,20 +621,27 @@
                 acc[there, cols] = tok[at, cols].astype(f32) + summed
 
     def block_near(unit):
-        send_hidden[unit].wait_recv()
-        passed[unit].wait_recv()
         here, there = lanes_of(unit)
         width = here.stop - here.start
         at = pl.ds(mine, 512)
-        left = jnp.concatenate([hidden[at, here], hidden_other[:, there]], axis=1)
+
+        def weight(ref, n, lanes):
+            return ref[n // 4, n % 4, :, :, lanes].reshape(256, width)
+
+        if unit == 4:
+            for n in range(8):
+                cols = slice(256 * n, 256 * n + 256)
+                acc[at, cols] = acc[at, cols] + dot_nt(hidden[at, here], weight(dn, n, here)) * sv_dn[n]
+        send_hidden[unit].wait_recv()
+        passed[unit].wait_recv()
         for n in range(8):
             cols = slice(256 * n, 256 * n + 256)
-            weights = [ref[n // 4, n % 4, :, :, lanes].reshape(256, width) for ref, lanes in ((dn, here), (dn_other, there))]
-            value = acc[at, cols] + dot_nt(left, jnp.concatenate(weights, axis=1)) * sv_dn[n]
-            if unit == 5:
-                out[:, cols] = value.astype(bf16)
+            if unit == 4:
+                acc[at, cols] = acc[at, cols] + dot_nt(hidden_other[:, there], weight(dn_other, n, there)) * sv_dn[n]
             else:
-                acc[at, cols] = value
+                left = jnp.concatenate([hidden[at, here], hidden_other[:, there]], axis=1)
+                right = jnp.concatenate([weight(dn, n, here), weight(dn_other, n, there)], axis=1)
+                out[:, cols] = (acc[at, cols] + dot_nt(left, right) * sv_dn[n]).astype(bf16)
 
     blocks = {
         "cast": block_cast,

time: 117 us -> 115 us (0.983)
  Pallas kernels: 117 us -> 115 us
    pallas_call x1, Pallas kernels: 116 us -> 113 us  [mega(): pl.pallas_call(lambda *refs: mega_kernel(ops, names, *refs), out_shape=pl...]
where the time goes in v6:
time: 115 us
  Pallas kernels  115 us (100%)
    pallas_call x1, Pallas kernels, mega(): pl.pallas_call(lambda *refs: mega_kernel(ops, names, *refs), out_shape=pl...  113 us

profile of v6, /device:TPU:1, one launch (start us, length us, event | category | flops | bytes accessed | tf_op | source)
XLA Modules:
  0.0 115.0 jit_solution(2399729250415937039)
XLA Ops:
  0.0 113.5 %shard_map.217.src = bf16[512,2048]{1,0:T(8,128)(2,1)S(1)} custom-call(bf16[512,2048]{1,0:T(8,128)(2,1)} %bitcast.4, f32[64,512]{1,0:T(8,128)} %refs_1_.1, f32[64,512]{1,0:T(8,128)} %refs_2_.1, f32[64,512]{1,0:T(8,128)} %refs_3_.1, f32[64,1408]{1,0:T(8,128)} %refs_4_.1, f32[64,1408]{1,0:T(8,128)} %refs_5_.1, f32[64,512]{1,0:T(8,128)} %bitcast.6, ...), custom_call_target="tpu_custom_call" | custom-call | tf_op jit(solution)/shard_map/pallas_call | solution.py:695
  113.5 1.3 %shard_map.218 = bf16[512,2048]{1,0:T(8,128)(2,1)} custom-call(bf16[512,2048]{1,0:T(8,128)(2,1)S(1)} %shard_map.217.src), custom_call_target="tpu_custom_call" | custom-call | tf_op jit(solution)/shard_map/pallas_call | solution.py:743
